TPU v7x, 256 devices: a whole 4x4x8 slice. The times are simulated.
256 devices in a mesh: sp: 32 (over z, x), tp: 8 (over y, core).
Axes of the slice: x: 4, y: 4, z: 8, core: 2. Of those that a mesh axis runs over, the one named last changes fastest.
Arguments:
- residual: bfloat16 [24576, 2048], P('sp'), may hold values from -6 to 6
- queries: bfloat16 [24576, 1024], P('sp', 'tp'), may hold values from -12 to 12
- keys: bfloat16 [24576, 512], P('sp', 'tp'), may hold values from -6 to 6
- values: bfloat16 [24576, 512], P('sp', 'tp'), may hold values from -36 to 36
- segments: int32 [24576], P('sp'), may hold values from 0 to 15, never falling along the last dimension, each value on 1 to 3072 neighbouring positions
- sink: float32 [16], P('tp'), may hold values from 3 to 7
- out_weight: bfloat16 [1024, 2048], replicated, may hold values from -0.1875 to 0.1875
- norm_gain_one: float32 [2048], replicated, may hold values from 0.1 to 1.9
- group: int32 [24576], P('sp'), may hold values from 0 to 3, as said below
- member: int32 [24576, 2], P('sp'), may hold values from 0 to 7, as said below
- route_weight: float32 [24576, 2], P('sp'), may hold values from 0.25 to 1
- gate_weight: bfloat16 [32, 2048, 1024], P('sp', None, 'tp'), may hold values from -0.125 to 0.125
- up_weight: bfloat16 [32, 2048, 1024], P('sp', None, 'tp'), may hold values from -0.125 to 0.125
- down_weight: bfloat16 [32, 1024, 2048], P('sp', None, 'tp'), may hold values from -0.1875 to 0.1875
- norm_gain_two: float32 [2048], P('tp'), may hold values from 0.1 to 1.9
Outputs:
- output: bfloat16 [24576, 2048], P('sp', 'tp')
Inputs may be any that keep to these rules, and one draw needn't show every extreme that they name: In every aligned block of 96 rows no expert (group * 8 + member) is named by more than 12 rows, and one expert, the same in all blocks of a draw, is named by exactly 12 rows of every block. `member`: the 2 members of a row differ.
All inputs are finite; a program needn't handle non-finite values.
Results may differ from a plain program's by a relative error of at most 0.0059.
Values may be sent and summed in bfloat16 or wider, within the bound.
No kernel may reach another device: no remote copies, remote signals or barrier semaphores. Data moves between devices by JAX's collectives and lax.ppermute only.
A program may use at most 128 MiB of HBM per device.

v0:
```python
import jax
import jax.numpy as jnp
from jax import lax
from jax.experimental import pallas as pl
from jax.experimental.pallas import tpu as pltpu
from jax.sharding import PartitionSpec as P


HEAD_DIM = 64
HALF = 128
PER_GROUP = 8
ALPHA = 2.0**0.25
EPS = 1e-05
NEG = -1e30
F32 = jnp.float32
BF16 = jnp.bfloat16

ROWS = 768
QB = 128
BLOCKS = ROWS // QB
TP = 8
BLK = ROWS // TP
CAP = 12
D = 2048
FF = 1024
SPX = 4
SPZ = 8
GROUP = 8
HALF_CAP = GROUP * CAP // 2
WIDE = D + 128
PICK = 2 * CAP
CHUNK = GROUP * PICK


def dot(a, b):
    return jnp.dot(a, b, preferred_element_type=F32)


def params(mib):
    return pltpu.CompilerParams(vmem_limit_bytes=mib * 1024 * 1024)


def iota(shape, dim):
    return lax.broadcasted_iota(jnp.int32, shape, dim)


VMEM = pl.BlockSpec(memory_space=pltpu.VMEM)
SMEM = pl.BlockSpec(memory_space=pltpu.SMEM)
HBM = pl.BlockSpec(memory_space=pltpu.HBM)


def in_hbm(*arrays):
    return [pltpu.with_memory_space_constraint(a, pltpu.HBM) for a in arrays]


def pack_kernel(q, k, v, s, gate, up, down, low, high, head, tail, qv, kt, vt, seg, held, sems):
    moves = [
        (k, kt),
        (v, vt),
        (s, seg),
        (gate.at[0], held.at[0, 0:D]),
        (up.at[0, 0:FF], held.at[0, D : D + FF]),
        (up.at[0, FF:D], held.at[1, 0:FF]),
        (down.at[0, :, 0:128], held.at[1, FF:D]),
        (down.at[0, :, 128:256], held.at[1, D : D + FF]),
        (q, qv),
    ]
    copies = [pltpu.make_async_copy(a, b, sems.at[n]) for n, (a, b) in enumerate(moves)]
    for copy in copies:
        copy.start()
    for copy in copies[:3]:
        copy.wait()
    for out, start, row in ((low, 0, 0), (high, ROWS - HALF, BLOCKS - 1)):
        out[0:64, :] = kt[:, start : start + HALF]
        out[64:128, :] = vt[:, start : start + HALF]
        out[128:144, :] = jnp.broadcast_to((seg[row : row + 1, :] + 1).astype(F32), (16, HALF)).astype(BF16)
    for copy in copies[3:8]:
        copy.wait()
    stores = [pltpu.make_async_copy(held.at[n], out, sems.at[9 + n]) for n, out in enumerate((head, tail))]
    for store in stores:
        store.start()
    for store in stores:
        store.wait()
    copies[8].wait()


def attend(q, kt, vt, seg_q, seg_k, sink):
    qs = jnp.concatenate([q[:, :HEAD_DIM], q[:, HEAD_DIM:]], axis=0)
    scores = dot(qs, kt) * HEAD_DIM ** (-0.5)
    col = jnp.transpose(jnp.broadcast_to(seg_q, (QB, QB)))
    row_i = iota((QB, QB), 0)
    col_i = iota((QB, QB), 1)
    parts = []
    for n, band in enumerate((col_i >= row_i, None, col_i <= row_i)):
        same = col == jnp.broadcast_to(seg_k[n], (QB, QB))
        parts.append(same if band is None else jnp.logical_and(same, band))
    allowed = jnp.concatenate(parts, axis=1)
    outs = []
    for h in range(2):
        part = jnp.where(allowed, scores[h * QB : (h + 1) * QB], NEG)
        peak = jnp.maximum(jnp.max(part, -1, keepdims=True), sink[h])
        raised = jnp.where(allowed, jnp.exp(part - peak), 0.0)
        denominator = jnp.sum(raised, -1, keepdims=True) + jnp.exp(sink[h] - peak)
        outs.append((raised / denominator).astype(BF16))
    weights = jnp.concatenate(outs, axis=0)
    got = lax.dot_general(weights, vt, (((1,), (1,)), ((), ())), preferred_element_type=F32)
    return jnp.concatenate([got[:QB], got[QB:]], axis=1).astype(BF16)


def interior_kernel(sink, q, kt, vt, seg, out):
    sinks = [jnp.full((QB, 1), sink[h], F32) for h in range(2)]
    rows = [(seg[b : b + 1, :] + 1).astype(F32) for b in range(BLOCKS)]
    for b in range(1, BLOCKS - 1):
        lo = (b - 1) * QB
        out[b * QB : (b + 1) * QB, :] = attend(
            q[b * QB : (b + 1) * QB, :],
            kt[:, lo : lo + 3 * QB],
            vt[:, lo : lo + 3 * QB],
            rows[b],
            rows[b - 1 : b + 2],
            sinks,
        )


def edge_kernel(sink, q, kt, vt, seg, before, after, part, out):
    sinks = [jnp.full((QB, 1), sink[h], F32) for h in range(2)]
    rows = [(seg[b : b + 1, :] + 1).astype(F32) for b in range(BLOCKS)]
    out[QB : ROWS - QB, :] = part[QB : ROWS - QB, :]
    out[:QB, :] = attend(
        q[:QB, :],
        jnp.concatenate([before[0:64, :], kt[:, : 2 * QB]], axis=1),
        jnp.concatenate([before[64:128, :], vt[:, : 2 * QB]], axis=1),
        rows[0],
        [before[128:129, :].astype(F32), rows[0], rows[1]],
        sinks,
    )
    lo = ROWS - QB
    out[lo:, :] = attend(
        q[lo:, :],
        jnp.concatenate([kt[:, lo - QB :], after[0:64, :]], axis=1),
        jnp.concatenate([vt[:, lo - QB :], after[64:128, :]], axis=1),
        rows[BLOCKS - 1],
        [rows[BLOCKS - 2], rows[BLOCKS - 1], after[128:129, :].astype(F32)],
        sinks,
    )


def routing_kernel(where, group, member, weight, residual, rows, cols, table_out, own_out, sem):
    place, z = where[0], where[1]
    start = pl.multiple_of(place * BLK, BLK)
    own_copy = pltpu.make_async_copy(residual.at[pl.ds(start, BLK), :], own_out, sem)
    own_copy.start()
    r0 = iota((BLK, BLK), 0)
    r1 = iota((BLK, BLK), 1)
    eye = r0 == r1
    own = iota((BLK, ROWS), 1) == iota((BLK, ROWS), 0) + place * BLK

    def column(row):
        return jnp.sum(jnp.where(own, jnp.broadcast_to(row, (BLK, ROWS)), 0.0), axis=1, keepdims=True)

    def turned(col):
        return jnp.sum(jnp.where(eye, jnp.broadcast_to(col, (BLK, BLK)), 0.0), axis=0, keepdims=True)

    def before(row, col):
        hit = jnp.logical_and(row == col, r1 < r0)
        return jnp.sum(jnp.where(hit, 1.0, 0.0), axis=1, keepdims=True)

    group_col = column(group[...].astype(F32))
    group_row = turned(group_col)
    away = (group_col.astype(jnp.int32) - (z >> 1)) & 3
    near = jnp.where((z & 1) == 0, 3, 1)
    way = jnp.where(away == 0, 0, jnp.where(away == 2, 3, jnp.where(away == near, 1, 2)))
    where_to = way.astype(F32) * HALF_CAP + before(group_row, group_col)
    cols[...] = jnp.broadcast_to(where_to, (BLK, 128))
    rows[...] = jnp.broadcast_to(turned(where_to), (8, BLK))

    member_cols = [column(member[k : k + 1, :].astype(F32)) for k in range(2)]
    id_cols = [group_col * PER_GROUP + m for m in member_cols]
    id_rows = [turned(c) for c in id_cols]
    entries = []
    for k in range(2):
        rank = before(id_rows[0], id_cols[k]) + before(id_rows[1], id_cols[k])
        entries.append(member_cols[k] * PICK + rank + 1.0)
    for k in range(2):
        rest = column(weight[k : k + 1, :])
        for _ in range(3):
            part = rest.astype(BF16).astype(F32)
            entries.append(part)
            rest = rest - part
    lane = iota((BLK, 128), 1)
    table = jnp.zeros((BLK, 128), F32)
    for n, c in enumerate(entries):
        table = jnp.where(lane == n, c, table)
    table_out[...] = table.astype(BF16)
    own_copy.wait()


def project_kernel(att, weight, residual, gain, rows, table, normed_out, *refs):
    sent, matrix, sems = refs[:-2], refs[-2], refs[-1]
    copies = [
        pltpu.make_async_copy(weight.at[n * 256 : (n + 1) * 256, :], matrix.at[n], sems.at[n]) for n in range(4)
    ]
    for copy in copies:
        copy.start()
    summed = ALPHA * residual[...].astype(F32)
    for n, copy in enumerate(copies):
        copy.wait()
        summed += dot(jnp.concatenate([att[2 * n], att[2 * n + 1]], axis=1), matrix[n])
    mean_value = jnp.mean(summed, -1, keepdims=True)
    variance = jnp.mean(jnp.square(summed - mean_value), -1, keepdims=True)
    normed = ((summed - mean_value) * lax.rsqrt(variance + EPS) * gain[...]).astype(BF16)
    normed_out[...] = normed
    slot = iota((4 * HALF_CAP, BLK), 0).astype(F32)
    chosen = jnp.where(slot == rows[0:1, :], 1.0, 0.0).astype(BF16)
    picked = dot(chosen, normed).astype(BF16)
    tables = dot(chosen, table[...]).astype(BF16)
    for n, out in enumerate(sent):
        out[:, :D] = picked[n * HALF_CAP : (n + 1) * HALF_CAP]
        out[:, D:] = tables[n * HALF_CAP : (n + 1) * HALF_CAP]


def expand_kernel(first, second, out, table_out):
    eye = iota((HALF_CAP, HALF_CAP), 0) == iota((HALF_CAP, HALF_CAP), 1)
    slot = iota((CHUNK, HALF_CAP), 0).astype(F32)
    chosen = []
    for n, a in enumerate((first, second)):
        table = a[:, D:]
        table_out[n * HALF_CAP : (n + 1) * HALF_CAP, :] = table
        hit = None
        for k in range(2):
            col = table[:, k : k + 1].astype(F32)
            row = jnp.sum(jnp.where(eye, jnp.broadcast_to(col, eye.shape), 0.0), axis=0, keepdims=True)
            target = jnp.where(row > 0.5, row - 1.0 + n * CAP, -1.0)
            match = slot == target
            hit = match if hit is None else jnp.logical_or(hit, match)
        chosen.append(jnp.where(hit, 1.0, 0.0).astype(BF16))
    out[...] = (dot(chosen[0], first[:, :D]) + dot(chosen[1], second[:, :D])).astype(BF16)


def expert_kernel(order, x, *refs):
    weights, (out, gate, up, down, hidden, sems) = refs[: 2 * TP], refs[2 * TP :]
    moves = []
    for n in range(TP):
        head, tail = weights[2 * n], weights[2 * n + 1]
        moves.append((head.at[0:D, :], gate.at[n]))
        moves.append((head.at[D:, :], up.at[n, 0:FF]))
        moves.append((tail.at[0:FF, :], up.at[n, FF:D]))
    for n in range(TP):
        moves.append((weights[2 * n + 1].at[FF:, :], down.at[n]))
    copies = [pltpu.make_async_copy(a, b, sems.at[n]) for n, (a, b) in enumerate(moves)]
    for copy in copies:
        copy.start()
    for n in range(TP):
        for copy in copies[3 * n : 3 * n + 3]:
            copy.wait()
        both = dot(x[...], jnp.concatenate([gate[n], up[n]], axis=1))
        hidden[order[n]] = (jax.nn.silu(both[:, :128]) * both[:, 128:]).astype(BF16)
    units = jnp.concatenate([hidden[n] for n in range(TP)], axis=1)
    for n in range(TP):
        copies[3 * TP + n].wait()
        columns = jnp.concatenate([down[n, :FF, :], down[n, FF:, :]], axis=1)
        out[:, pl.ds(pl.multiple_of(order[n] * 256, 256), 256)] = dot(units, columns).astype(BF16)


def shrink_kernel(produced, table, first, second):
    count = 2 * HALF_CAP
    slot = iota((count, CHUNK), 1).astype(F32)
    origin = jnp.where(iota((count, 1), 0) >= HALF_CAP, float(CAP), 0.0)
    entries = table[...].astype(F32)
    total = jnp.zeros((count, D), F32)
    for k in range(2):
        col = entries[:, k : k + 1]
        target = jnp.where(col > 0.5, col - 1.0 + origin, -1.0)
        chosen = jnp.where(slot == target, 1.0, 0.0).astype(BF16)
        at = 2 + 3 * k
        weight = (entries[:, at : at + 1] + entries[:, at + 1 : at + 2]) + entries[:, at + 2 : at + 3]
        total += weight * dot(chosen, produced[...])
    first[...] = total[:HALF_CAP].astype(BF16)
    second[...] = total[HALF_CAP:].astype(BF16)


def combine_kernel(normed, cols, own, a, b, c, out):
    slot = iota((BLK, 4 * HALF_CAP), 1).astype(F32)
    chosen = jnp.where(slot == cols[:, 0:1], 1.0, 0.0).astype(BF16)
    stacked = jnp.concatenate([own[...], a[...], b[...], c[...]], axis=0)
    summed = ALPHA * normed[...].astype(F32) + dot(chosen, stacked)
    mean_value = jnp.mean(summed, -1, keepdims=True)
    variance = jnp.mean(jnp.square(summed - mean_value), -1, keepdims=True)
    scaled = (summed - mean_value) * lax.rsqrt(variance + EPS)
    width = out.shape[2]
    for n in range(out.shape[0]):
        out[n] = scaled[:, n * width : (n + 1) * width].astype(BF16)


def kernel(body, mib, outs, spaces, *operands, scratch=()):
    return pl.pallas_call(
        body,
        out_shape=outs,
        in_specs=spaces,
        out_specs=[VMEM] * len(outs),
        scratch_shapes=list(scratch),
        compiler_params=params(mib),
    )(*operands)


def layer(
    residual,
    queries,
    keys,
    values,
    segments,
    sink,
    out_weight,
    norm_gain_one,
    group,
    member,
    route_weight,
    gate_weight,
    up_weight,
    down_weight,
    norm_gain_two,
):
    place = lax.axis_index("tp")
    sp_place = lax.axis_index("sp")
    kt = keys.T
    vt = values.T
    seg = segments.reshape(BLOCKS, QB)
    halo = jax.ShapeDtypeStruct((144, HALF), BF16)
    packed_shape = pltpu.HBM((D + FF, 128), BF16)
    local = [jax.ShapeDtypeStruct(a.shape, a.dtype) for a in (queries, kt, vt, seg)]
    low, high, head, tail, queries, kt, vt, seg = pl.pallas_call(
        pack_kernel,
        out_shape=(halo, halo, packed_shape, packed_shape, *local),
        in_specs=[HBM] * 7,
        out_specs=(VMEM, VMEM, HBM, HBM) + (VMEM,) * 4,
        scratch_shapes=[pltpu.VMEM((2, D + FF, 128), BF16), pltpu.SemaphoreType.DMA((11,))],
        compiler_params=params(8),
        name="pack",
    )(*in_hbm(queries, kt, vt, seg, gate_weight, up_weight, down_weight))
    sp = SPX * SPZ
    forward = [(i, i + 1) for i in range(sp - 1)]
    before = lax.ppermute(high, "sp", forward)
    after = lax.ppermute(low, "sp", [(t, s) for s, t in forward])

    def along_y(array, shift):
        pairs = [(y * 2 + c, (y + shift) % 4 * 2 + c) for y in range(4) for c in range(2)]
        return lax.ppermute(array, "tp", pairs)

    def swapped(array):
        return lax.ppermute(array, "tp", [(n, n ^ 1) for n in range(TP)])

    from_low, from_high = along_y(head, 1), along_y(head, -1)
    tail_low, tail_high = along_y(tail, 1), along_y(tail, -1)
    head_far = along_y(from_low, 1)
    tail_far = along_y(tail_high, -1)
    other_heads = [swapped(a) for a in (head, from_low, from_high)]
    other_tails = [swapped(a) for a in (tail, tail_low, tail_high)]
    other_heads.append(swapped(head_far))
    other_tails.append(swapped(tail_far))
    heads_all = [head, from_low, from_high, head_far] + other_heads
    tails_all = [tail, tail_low, tail_high, tail_far] + other_tails
    weights = [a for pair in zip(heads_all, tails_all) for a in pair]

    rows_shape = jax.ShapeDtypeStruct((ROWS, 128), BF16)
    interior = pl.pallas_call(
        interior_kernel,
        out_shape=rows_shape,
        in_specs=[SMEM] + [VMEM] * 4,
        out_specs=VMEM,
        compiler_params=params(8),
        name="interior",
    )(sink, queries, kt, vt, seg)

    where = jnp.stack([place, sp_place >> 2]).astype(jnp.int32)
    rows, cols, table, own_residual = kernel(
        routing_kernel,
        12,
        (
            jax.ShapeDtypeStruct((8, BLK), F32),
            jax.ShapeDtypeStruct((BLK, 128), F32),
            jax.ShapeDtypeStruct((BLK, 128), BF16),
            jax.ShapeDtypeStruct((BLK, D), BF16),
        ),
        [SMEM] + [VMEM] * 3 + [HBM],
        where,
        group.reshape(1, ROWS),
        member.T,
        route_weight.T,
        *in_hbm(residual),
        scratch=[pltpu.SemaphoreType.DMA(())],
    )

    operands = (queries, kt, vt, seg, before, after, interior)
    attended = pl.pallas_call(
        edge_kernel,
        out_shape=rows_shape,
        in_specs=[SMEM] + [VMEM] * len(operands),
        out_specs=VMEM,
        compiler_params=params(8),
        name="edges",
    )(sink, *operands)

    heads = lax.all_to_all(attended.reshape(TP, BLK, 128), "tp", 0, 0, tiled=True)

    normed, *sent = kernel(
        project_kernel,
        24,
        [jax.ShapeDtypeStruct((BLK, D), BF16)] + [jax.ShapeDtypeStruct((HALF_CAP, WIDE), BF16)] * 4,
        [VMEM, HBM] + [VMEM] * 4,
        heads,
        *in_hbm(out_weight),
        own_residual,
        norm_gain_one.reshape(1, D),
        rows,
        table,
        scratch=[pltpu.VMEM((4, 256, D), BF16), pltpu.SemaphoreType.DMA((4,))],
    )

    def along_z(array, even, odd):
        step = (even, odd)
        pairs = [(z * SPX + x, (z + step[z % 2]) % SPZ * SPX + x) for z in range(SPZ) for x in range(SPX)]
        return lax.ppermute(array, "sp", pairs)

    def in_group(array):
        groups = [[g * GROUP + n for n in range(GROUP)] for g in range(sp // GROUP)]
        split = array.reshape(GROUP, PICK, D)
        moved = lax.all_to_all(split, "sp", 0, 0, axis_index_groups=groups, tiled=True)
        return moved.reshape(CHUNK, D)

    piece = jax.ShapeDtypeStruct((CHUNK, D), BF16)

    def spread(first, second):
        out = (piece, jax.ShapeDtypeStruct((2 * HALF_CAP, 128), BF16))
        rows, tables = kernel(expand_kernel, 12, out, [VMEM] * 2, first, second)
        return in_group(rows), tables

    def shrink(produced, tables):
        out = [jax.ShapeDtypeStruct((HALF_CAP, D), BF16)] * 2
        return kernel(shrink_kernel, 12, out, [VMEM] * 2, in_group(produced), tables)

    near = along_z(sent[1], -1, 1)
    other = along_z(sent[2], 2, -2)
    far = along_z(sent[3], -3, 3)
    rows_one, tables_one = spread(sent[0], near)
    rows_two, tables_two = spread(other, far)

    away = jnp.array([0, -2, 2, 4], jnp.int32)
    order = (jnp.concatenate([place + away, (place ^ 1) + away]) & 7).astype(jnp.int32)

    def apply(rows):
        return kernel(
            expert_kernel,
            24,
            (piece,),
            [SMEM, VMEM] + [HBM] * (2 * TP),
            order,
            rows,
            *in_hbm(*weights),
            scratch=[
                pltpu.VMEM((TP, D, 128), BF16),
                pltpu.VMEM((TP, D, 128), BF16),
                pltpu.VMEM((TP, D, 128), BF16),
                pltpu.VMEM((TP, CHUNK, 128), BF16),
                pltpu.SemaphoreType.DMA((4 * TP,)),
            ],
        )[0]

    made_one = apply(rows_one)
    made_two = apply(rows_two)
    back_two = shrink(made_two, tables_two)
    back_one = shrink(made_one, tables_one)
    back = [*back_one, *back_two]

    (scaled,) = kernel(
        combine_kernel,
        16,
        (jax.ShapeDtypeStruct((TP, BLK, D // TP), BF16),),
        [VMEM] * 6,
        normed,
        cols,
        back[0],
        along_z(back[1], -1, 1),
        along_z(back[2], -2, 2),
        along_z(back[3], -3, 3),
    )

    last = lax.all_to_all(scaled, "tp", 0, 0, tiled=True).reshape(ROWS, D // TP)
    return (last.astype(F32) * norm_gain_two).astype(BF16)


def solution(mesh):
    in_specs = (
        P("sp", None),
        P("sp", "tp"),
        P("sp", "tp"),
        P("sp", "tp"),
        P("sp"),
        P("tp"),
        P(),
        P(),
        P("sp"),
        P("sp", None),
        P("sp", None),
        P("sp", None, "tp"),
        P("sp", None, "tp"),
        P("sp", None, "tp"),
        P("tp"),
    )
    out_specs = P("sp", "tp")
    return jax.shard_map(layer, mesh=mesh, in_specs=in_specs, out_specs=out_specs, check_vma=False)
```

profile of v0, /device:TPU:1, one launch (start us, length us, event | category | flops | bytes accessed | tf_op | source)
XLA Modules:
  0.0 180.8 jit_solution(4707175581627271871)
XLA Ops:
  0.0 2.7 %pack.1 = (bf16[144,128]{1,0:T(8,128)(2,1)S(1)}, bf16[144,128]{1,0:T(8,128)(2,1)S(1)}, bf16[3072,128]{1,0:T(8,128)(2,1)}, bf16[3072,128]{1,0:T(8,128)(2,1)}, bf1...) custom-call(bf16[768,128]{1,0:T(8,128)(2,1)} %q.1, ...), custom_call_target="tpu_custom_call" | custom-call | tf_op jit(solution)/shard_map/pack/pallas_call | solution.py:331
  2.8 3.9 %collective-permute-start = (bf16[144,128]{1,0:T(8,128)(2,1)S(1)}, bf16[144,128]{1,0:T(8,128)(2,1)S(1)}, u32[]{:S(2)}, u32[]{:S(2)}) collective-permute-start(bf16[144,128]{1,0:T(8,128)(2,1)S(1)} %get-tuple-element.34), channel_id=1, source_target_pairs={{0,8},{8,16},{16,24},{24,32},{32,40},{40,48},{48,56},{56,64},{64,7... | collective-permute-start | bytes 110600 | tf_op jit(solution)/shard_map/ppermute | solution.py:342
  6.7 1.3 collective-permute-start.1
  8.0 0.0 copy-start.3
  8.0 0.6 copy-done.3
  8.7 2.4 %interior.1.part = bf16[768,128]{1,0:T(8,128)(2,1)S(1)} custom-call(f32[2]{0:T(128)S(1)} %copy-done.3, bf16[768,128]{1,0:T(8,128)(2,1)S(1)} %get-tuple-element.30.q, bf16[64,768]{1,0:T(8,128)(2,1)S(1)} %get-tuple-element.31.kt, bf16[64,768]{1,0:T(8,128)(2,1)S(1)} %get-tuple-element.32.vt, s32[6,128]{1,0:T(8,128)S(1)} %get-tuple-element.33.seg), custom_call_target="tpu_custom_call" | custom-call | tf_op jit(solution)/shard_map/interior/pallas_call | solution.py:365
  11.1 0.3 collective-permute-done.1.after
  11.4 2.3 %edges.1 = bf16[768,128]{1,0:T(8,128)(2,1)} custom-call(f32[2]{0:T(128)S(1)} %copy-done.3, bf16[768,128]{1,0:T(8,128)(2,1)S(1)} %get-tuple-element.30.q, bf16[64,768]{1,0:T(8,128)(2,1)S(1)} %get-tuple-element.31.kt, bf16[64,768]{1,0:T(8,128)(2,1)S(1)} %get-tuple-element.32.vt, s32[6,128]{1,0:T(8,128)S(1)} %get-tuple-element.33.seg, ...), custom_call_target="tpu_custom_call" | custom-call | tf_op jit(solution)/shard_map/edges/pallas_call | solution.py:394
  13.7 6.6 %all-to-all-start = ((bf16[8,96,128]{2,1,0:T(8,128)(2,1)}), bf16[8,96,128]{2,1,0:T(8,128)(2,1)S(1)}, u32[]{:S(2)}, u32[]{:S(2)}) async-start(bf16[8,96,128]{2,1,0:T(8,128)(2,1)} %bitcast.3), calls=%async_computation | async-start | bytes 393216 | tf_op jit(solution)/shard_map/all_to_all | solution.py:403
  20.3 0.7 reshape.42.group
  20.9 0.1 pad_add_fusion.where
  21.0 0.7 copy-done.1
  21.7 0.7 copy-done.2
  22.4 1.8 shard_map.154
  24.2 1.9 %all-to-all-done.att = bf16[8,96,128]{2,1,0:T(8,128)(2,1)S(1)} async-done(((bf16[8,96,128]{2,1,0:T(8,128)(2,1)}), bf16[8,96,128]{2,1,0:T(8,128)(2,1)S(1)}, u32[]{:S(2)}, u32[]{:S(2)}) %all-to-all-start) | async-done | bytes 196640 | tf_op jit(solution)/shard_map/all_to_all | solution.py:403
  26.1 3.1 %shard_map.155 = (bf16[96,2048]{1,0:T(8,128)(2,1)S(1)}, bf16[48,2176]{1,0:T(8,128)(2,1)S(1)}, bf16[48,2176]{1,0:T(8,128)(2,1)S(1)}, bf16[48,2176]{1,0:T(8,128)(2,1)S(1)}, bf16[48,2176]{1,0:T(8,128)(2,1)S(1)}) custom-call(bf16[8,96,128]{2,1,0:T(8,128)(2,1)S(1)} %all-to-all-done.att, bf16[1024,2048]{1,0:T(8,128)(2,1)} %weight.1, ...), custom_call_target="tpu_custom_call" | custom-call | tf_op jit(solution)/shard_map/pallas_call | solution.py:296
  29.3 7.5 %collective-permute-start.2 = (bf16[48,2176]{1,0:T(8,128)(2,1)S(1)}, bf16[48,2176]{1,0:T(8,128)(2,1)S(1)}, u32[]{:S(2)}, u32[]{:S(2)}) collective-permute-start(bf16[48,2176]{1,0:T(8,128)(2,1)S(1)} %get-tuple-element.42), channel_id=1, source_target_pairs={{0,224},{8,232},{16,240},{24,248},{32,64},{40,72},{48,80},{56,88},... | collective-permute-start | bytes 626696 | tf_op jit(solution)/shard_map/ppermute | solution.py:422
  36.7 4.6 %collective-permute-done.2.second = bf16[48,2176]{1,0:T(8,128)(2,1)S(1)} collective-permute-done((bf16[48,2176]{1,0:T(8,128)(2,1)S(1)}, bf16[48,2176]{1,0:T(8,128)(2,1)S(1)}, u32[]{:S(2)}, u32[]{:S(2)}) %collective-permute-start.2) | collective-permute-done | bytes 208928 | tf_op jit(solution)/shard_map/ppermute | solution.py:422
  41.3 1.5 shard_map.156
  42.9 3.5 %all-to-all-start.1 = ((bf16[8,24,2048]{2,1,0:T(8,128)(2,1)}), bf16[8,24,2048]{2,1,0:T(8,128)(2,1)S(1)}, u32[]{:S(2)}, u32[]{:S(2)}) async-start(bf16[8,24,2048]{2,1,0:T(8,128)(2,1)} %bitcast.9), calls=%async_computation.1 | async-start | bytes 1572864 | tf_op jit(solution)/shard_map/all_to_all | solution.py:427
  46.4 0.3 collective-permute-start.3
  46.8 1.0 collective-permute-start.4
  47.8 1.6 collective-permute-start.6
  49.4 1.2 collective-permute-start.5
  50.6 4.4 %collective-permute-start.18 = (bf16[48,2176]{1,0:T(8,128)(2,1)S(1)}, bf16[48,2176]{1,0:T(8,128)(2,1)S(1)}, u32[]{:S(2)}, u32[]{:S(2)}) collective-permute-start(bf16[48,2176]{1,0:T(8,128)(2,1)S(1)} %get-tuple-element.49), channel_id=1, source_target_pairs={{0,64},{8,72},{16,80},{24,88},{32,224},{40,232},{48,240},{56,248},... | collective-permute-start | bytes 626696 | tf_op jit(solution)/shard_map/ppermute | solution.py:422
  55.0 5.2 %collective-permute-done.18.first = bf16[48,2176]{1,0:T(8,128)(2,1)S(1)} collective-permute-done((bf16[48,2176]{1,0:T(8,128)(2,1)S(1)}, bf16[48,2176]{1,0:T(8,128)(2,1)S(1)}, u32[]{:S(2)}, u32[]{:S(2)}) %collective-permute-start.18) | collective-permute-done | bytes 208928 | tf_op jit(solution)/shard_map/ppermute | solution.py:422
  60.2 2.8 %collective-permute-start.19 = (bf16[48,2176]{1,0:T(8,128)(2,1)S(1)}, bf16[48,2176]{1,0:T(8,128)(2,1)S(1)}, u32[]{:S(2)}, u32[]{:S(2)}) collective-permute-start(bf16[48,2176]{1,0:T(8,128)(2,1)S(1)} %get-tuple-element.50), channel_id=1, source_target_pairs={{0,160},{8,168},{16,176},{24,184},{32,128},{40,136},{48,144},{56,1... | collective-permute-start | bytes 626696 | tf_op jit(solution)/shard_map/ppermute | solution.py:422
  63.0 6.2 %collective-permute-done.19.second = bf16[48,2176]{1,0:T(8,128)(2,1)S(1)} collective-permute-done((bf16[48,2176]{1,0:T(8,128)(2,1)S(1)}, bf16[48,2176]{1,0:T(8,128)(2,1)S(1)}, u32[]{:S(2)}, u32[]{:S(2)}) %collective-permute-start.19) | collective-permute-done | bytes 208928 | tf_op jit(solution)/shard_map/ppermute | solution.py:422
  69.2 5.4 %collective-permute-start.9 = (bf16[3072,128]{1,0:T(8,128)(2,1)S(1)}, bf16[3072,128]{1,0:T(8,128)(2,1)}, u32[]{:S(2)}, u32[]{:S(2)}) collective-permute-start(bf16[3072,128]{1,0:T(8,128)(2,1)S(1)} %copy-done.4), channel_id=1, source_target_pairs={{0,1},{1,0},{2,3},{3,2},{4,5},{5,4},{6,7},{7,6},{8,9},{9,8},{10,11... | collective-permute-start | bytes 2359304 | tf_op jit(solution)/shard_map/ppermute | solution.py:350
  74.6 0.0 collective-permute-done.3.refs_2_
  74.6 0.0 collective-permute-start.10
  74.6 7.6 %collective-permute-done.4.refs_3_ = bf16[3072,128]{1,0:T(8,128)(2,1)} collective-permute-done((bf16[3072,128]{1,0:T(8,128)(2,1)}, bf16[3072,128]{1,0:T(8,128)(2,1)}, u32[]{:S(2)}, u32[]{:S(2)}) %collective-permute-start.4) | collective-permute-done | bytes 786464 | tf_op jit(solution)/shard_map/ppermute | solution.py:347
  82.2 0.0 collective-permute-start.7
  82.2 2.7 %collective-permute-start.8 = (bf16[3072,128]{1,0:T(8,128)(2,1)}, bf16[3072,128]{1,0:T(8,128)(2,1)}, u32[]{:S(2)}, u32[]{:S(2)}) collective-permute-start(bf16[3072,128]{1,0:T(8,128)(2,1)} %collective-permute-done.6.refs_5_), channel_id=1, source_target_pairs={{0,6},{1,7},{2,0},{3,1},{4,2},{5,3},{6,4},{7,5},{8,14},{9,15},{10,... | collective-permute-start | bytes 2359304 | tf_op jit(solution)/shard_map/ppermute | solution.py:347
  84.9 2.9 %collective-permute-start.11 = (bf16[3072,128]{1,0:T(8,128)(2,1)}, bf16[3072,128]{1,0:T(8,128)(2,1)}, u32[]{:S(2)}, u32[]{:S(2)}) collective-permute-start(bf16[3072,128]{1,0:T(8,128)(2,1)} %collective-permute-done.3.refs_2_), channel_id=1, source_target_pairs={{0,1},{1,0},{2,3},{3,2},{4,5},{5,4},{6,7},{7,6},{8,9},{9,8},{10,11... | collective-permute-start | bytes 2359304 | tf_op jit(solution)/shard_map/ppermute | solution.py:350
  87.9 1.5 shard_map.159
  89.4 5.0 %all-to-all-start.3 = ((bf16[8,24,2048]{2,1,0:T(8,128)(2,1)}), bf16[8,24,2048]{2,1,0:T(8,128)(2,1)S(1)}, u32[]{:S(2)}, u32[]{:S(2)}) async-start(bf16[8,24,2048]{2,1,0:T(8,128)(2,1)} %bitcast.13), calls=%async_computation.3 | async-start | bytes 1572864 | tf_op jit(solution)/shard_map/all_to_all | solution.py:427
  94.4 0.4 collective-permute-start.14
  94.7 0.2 collective-permute-start.12
  95.0 5.5 %collective-permute-done.7.refs_6_ = bf16[3072,128]{1,0:T(8,128)(2,1)} collective-permute-done((bf16[3072,128]{1,0:T(8,128)(2,1)}, bf16[3072,128]{1,0:T(8,128)(2,1)}, u32[]{:S(2)}, u32[]{:S(2)}) %collective-permute-start.7) | collective-permute-done | bytes 786464 | tf_op jit(solution)/shard_map/ppermute | solution.py:347
  100.5 3.2 %collective-permute-start.13 = (bf16[3072,128]{1,0:T(8,128)(2,1)}, bf16[3072,128]{1,0:T(8,128)(2,1)}, u32[]{:S(2)}, u32[]{:S(2)}) collective-permute-start(bf16[3072,128]{1,0:T(8,128)(2,1)} %collective-permute-done.5.refs_4_), channel_id=1, source_target_pairs={{0,1},{1,0},{2,3},{3,2},{4,5},{5,4},{6,7},{7,6},{8,9},{9,8},{10,11... | collective-permute-start | bytes 2359304 | tf_op jit(solution)/shard_map/ppermute | solution.py:350
  103.7 0.0 collective-permute-start.15
  103.7 0.5 collective-permute-start.16
  104.2 0.1 add_and_fusion.order
  104.3 1.6 collective-permute-done.13.refs_12_
  106.0 1.1 collective-permute-done.15.refs_14_
  107.1 1.1 collective-permute-done.16.refs_15_
  108.2 10.3 %shard_map.157 = bf16[192,2048]{1,0:T(8,128)(2,1)} custom-call(s32[8]{0:T(128)S(1)} %add_and_fusion.order, bf16[192,2048]{1,0:T(8,128)(2,1)S(1)} %bitcast.20, bf16[3072,128]{1,0:T(8,128)(2,1)} %get-tuple-element.44.refs_0_, bf16[3072,128]{1,0:T(8,128)(2,1)} %get-tuple-element.45.refs_1_, bf16[3072,128]{1,0:T(8,128)(2,1)} %collective-permute-done.3.refs_2_, ...), custom_call_target="tpu_custom_call" | custom-call | tf_op jit(solution)/shard_map/pallas_call | solution.py:296
  118.5 4.7 %all-to-all-start.2 = ((bf16[8,24,2048]{2,1,0:T(8,128)(2,1)}), bf16[8,24,2048]{2,1,0:T(8,128)(2,1)S(1)}, u32[]{:S(2)}, u32[]{:S(2)}) async-start(bf16[8,24,2048]{2,1,0:T(8,128)(2,1)} %bitcast.11), calls=%async_computation.2 | async-start | bytes 1572864 | tf_op jit(solution)/shard_map/all_to_all | solution.py:427
  123.2 10.3 %shard_map.160 = bf16[192,2048]{1,0:T(8,128)(2,1)} custom-call(s32[8]{0:T(128)S(1)} %add_and_fusion.order, bf16[192,2048]{1,0:T(8,128)(2,1)S(1)} %bitcast.21, bf16[3072,128]{1,0:T(8,128)(2,1)} %get-tuple-element.44.refs_0_, bf16[3072,128]{1,0:T(8,128)(2,1)} %get-tuple-element.45.refs_1_, bf16[3072,128]{1,0:T(8,128)(2,1)} %collective-permute-done.3.refs_2_, ...), custom_call_target="tpu_custom_call" | custom-call | tf_op jit(solution)/shard_map/pallas_call | solution.py:296
  133.5 0.0 copy-start.6
  133.5 1.6 all-to-all-done.2
  135.1 4.0 %all-to-all-start.4 = ((bf16[8,24,2048]{2,1,0:T(8,128)(2,1)}), bf16[8,24,2048]{2,1,0:T(8,128)(2,1)S(1)}, u32[]{:S(2)}, u32[]{:S(2)}) async-start(bf16[8,24,2048]{2,1,0:T(8,128)(2,1)} %bitcast.15), calls=%async_computation.4 | async-start | bytes 1572864 | tf_op jit(solution)/shard_map/all_to_all | solution.py:427
  139.0 0.4 shard_map.158
  139.5 1.5 collective-permute-start.17
  141.0 9.7 %all-to-all-done.4 = bf16[8,24,2048]{2,1,0:T(8,128)(2,1)S(1)} async-done(((bf16[8,24,2048]{2,1,0:T(8,128)(2,1)}), bf16[8,24,2048]{2,1,0:T(8,128)(2,1)S(1)}, u32[]{:S(2)}, u32[]{:S(2)}) %all-to-all-start.4) | async-done | bytes 786464 | tf_op jit(solution)/shard_map/all_to_all | solution.py:427
  150.7 0.4 shard_map.161
  151.1 1.2 collective-permute-start.20
  152.4 4.1 %collective-permute-start.21 = (bf16[48,2048]{1,0:T(8,128)(2,1)S(1)}, bf16[48,2048]{1,0:T(8,128)(2,1)S(1)}, u32[]{:S(2)}, u32[]{:S(2)}) collective-permute-start(bf16[48,2048]{1,0:T(8,128)(2,1)S(1)} %get-tuple-element.54), channel_id=1, source_target_pairs={{0,160},{8,168},{16,176},{24,184},{32,128},{40,136},{48,144},{56,1... | collective-permute-start | bytes 589832 | tf_op jit(solution)/shard_map/ppermute | solution.py:422
  156.5 2.6 %collective-permute-done.20.b = bf16[48,2048]{1,0:T(8,128)(2,1)S(1)} collective-permute-done((bf16[48,2048]{1,0:T(8,128)(2,1)S(1)}, bf16[48,2048]{1,0:T(8,128)(2,1)S(1)}, u32[]{:S(2)}, u32[]{:S(2)}) %collective-permute-start.20) | collective-permute-done | bytes 196640 | tf_op jit(solution)/shard_map/ppermute | solution.py:422
  159.1 7.0 %collective-permute-done.21.c = bf16[48,2048]{1,0:T(8,128)(2,1)S(1)} collective-permute-done((bf16[48,2048]{1,0:T(8,128)(2,1)S(1)}, bf16[48,2048]{1,0:T(8,128)(2,1)S(1)}, u32[]{:S(2)}, u32[]{:S(2)}) %collective-permute-start.21) | collective-permute-done | bytes 196640 | tf_op jit(solution)/shard_map/ppermute | solution.py:422
  166.1 0.6 shard_map.162
  166.7 13.3 %all_to_all.30 = bf16[8,96,256]{2,1,0:T(8,128)(2,1)S(1)} all-to-all(bf16[8,96,256]{2,1,0:T(8,128)(2,1)S(1)} %shard_map.162), channel_id=1, replica_groups=mesh['sp'=32,'tp'=8] {'tp'}, dimensions={0} | all-to-all | bytes 786432 | tf_op jit(solution)/shard_map/all_to_all | solution.py:487
  179.9 0.8 fusion
  (24 shorter events, 0.1 us)
Async XLA Ops:
  0.0 26.1 %copy-start = (f32[2048]{0:T(1024)S(1)}, f32[2048]{0:T(1024)}, u32[]{:S(2)}) copy-start(f32[2048]{0:T(1024)} %param.23) | copy-start | bytes 24580
  2.8 8.3 %collective-permute-start = (bf16[144,128]{1,0:T(8,128)(2,1)S(1)}, bf16[144,128]{1,0:T(8,128)(2,1)S(1)}, u32[]{:S(2)}, u32[]{:S(2)}) collective-permute-start(bf16[144,128]{1,0:T(8,128)(2,1)S(1)} %get-tuple-element.34), channel_id=1, source_target_pairs={{0,8},{8,16},{16,24},{24,32},{32,40},{40,48},{48,56},{56,64},{64,7... | collective-permute-start | bytes 110600 | tf_op jit(solution)/shard_map/ppermute | solution.py:342
  6.7 4.7 %collective-permute-start.1 = (bf16[144,128]{1,0:T(8,128)(2,1)S(1)}, bf16[144,128]{1,0:T(8,128)(2,1)S(1)}, u32[]{:S(2)}, u32[]{:S(2)}) collective-permute-start(bf16[144,128]{1,0:T(8,128)(2,1)S(1)} %get-tuple-element.35), channel_id=1, source_target_pairs={{8,0},{16,8},{24,16},{32,24},{40,32},{48,40},{56,48},{64,56},{72,6... | collective-permute-start | bytes 110600 | tf_op jit(solution)/shard_map/ppermute | solution.py:343
  8.0 0.7 copy-start.3
  13.7 12.4 %all-to-all-start = ((bf16[8,96,128]{2,1,0:T(8,128)(2,1)}), bf16[8,96,128]{2,1,0:T(8,128)(2,1)S(1)}, u32[]{:S(2)}, u32[]{:S(2)}) async-start(bf16[8,96,128]{2,1,0:T(8,128)(2,1)} %bitcast.3), calls=%async_computation | async-start | bytes 393216 | tf_op jit(solution)/shard_map/all_to_all | solution.py:403
  21.0 0.7 copy-start.1
  21.7 0.7 copy-start.2
  24.2 22.2 %copy-start.4 = (bf16[3072,128]{1,0:T(8,128)(2,1)S(1)}, bf16[3072,128]{1,0:T(8,128)(2,1)}, u32[]{:S(2)}) copy-start(bf16[3072,128]{1,0:T(8,128)(2,1)} %get-tuple-element.44.refs_0_) | copy-start | bytes 2359300
  26.1 78.1 %copy-start.7 = (s32[4]{0:T(128)S(1)}, s32[4]{0:T(128)}, u32[]{:S(2)}) copy-start(s32[4]{0:T(128)} %constant.17.clone) | copy-start | bytes 52
  29.3 12.1 %collective-permute-start.2 = (bf16[48,2176]{1,0:T(8,128)(2,1)S(1)}, bf16[48,2176]{1,0:T(8,128)(2,1)S(1)}, u32[]{:S(2)}, u32[]{:S(2)}) collective-permute-start(bf16[48,2176]{1,0:T(8,128)(2,1)S(1)} %get-tuple-element.42), channel_id=1, source_target_pairs={{0,224},{8,232},{16,240},{24,248},{32,64},{40,72},{48,80},{56,88},... | collective-permute-start | bytes 626696 | tf_op jit(solution)/shard_map/ppermute | solution.py:422
  42.9 46.5 %all-to-all-start.1 = ((bf16[8,24,2048]{2,1,0:T(8,128)(2,1)}), bf16[8,24,2048]{2,1,0:T(8,128)(2,1)S(1)}, u32[]{:S(2)}, u32[]{:S(2)}) async-start(bf16[8,24,2048]{2,1,0:T(8,128)(2,1)} %bitcast.9), calls=%async_computation.1 | async-start | bytes 1572864 | tf_op jit(solution)/shard_map/all_to_all | solution.py:427
  46.4 28.2 %collective-permute-start.3 = (bf16[3072,128]{1,0:T(8,128)(2,1)S(1)}, bf16[3072,128]{1,0:T(8,128)(2,1)}, u32[]{:S(2)}, u32[]{:S(2)}) collective-permute-start(bf16[3072,128]{1,0:T(8,128)(2,1)S(1)} %copy-done.4), channel_id=1, source_target_pairs={{0,2},{1,3},{2,4},{3,5},{4,6},{5,7},{6,0},{7,1},{8,10},{9,11},{10,... | collective-permute-start | bytes 2359304 | tf_op jit(solution)/shard_map/ppermute | solution.py:347
  46.8 35.5 %collective-permute-start.4 = (bf16[3072,128]{1,0:T(8,128)(2,1)}, bf16[3072,128]{1,0:T(8,128)(2,1)}, u32[]{:S(2)}, u32[]{:S(2)}) collective-permute-start(bf16[3072,128]{1,0:T(8,128)(2,1)} %get-tuple-element.45.refs_1_), channel_id=1, source_target_pairs={{0,2},{1,3},{2,4},{3,5},{4,6},{5,7},{6,0},{7,1},{8,10},{9,11},{10,... | collective-permute-start | bytes 2359304 | tf_op jit(solution)/shard_map/ppermute | solution.py:347
  47.8 34.5 %collective-permute-start.6 = (bf16[3072,128]{1,0:T(8,128)(2,1)}, bf16[3072,128]{1,0:T(8,128)(2,1)}, u32[]{:S(2)}, u32[]{:S(2)}) collective-permute-start(bf16[3072,128]{1,0:T(8,128)(2,1)} %get-tuple-element.45.refs_1_), channel_id=1, source_target_pairs={{0,6},{1,7},{2,0},{3,1},{4,2},{5,3},{6,4},{7,5},{8,14},{9,15},{10,... | collective-permute-start | bytes 2359304 | tf_op jit(solution)/shard_map/ppermute | solution.py:347
  49.4 35.5 %collective-permute-start.5 = (bf16[3072,128]{1,0:T(8,128)(2,1)S(1)}, bf16[3072,128]{1,0:T(8,128)(2,1)}, u32[]{:S(2)}, u32[]{:S(2)}) collective-permute-start(bf16[3072,128]{1,0:T(8,128)(2,1)S(1)} %copy-done.4), channel_id=1, source_target_pairs={{0,6},{1,7},{2,0},{3,1},{4,2},{5,3},{6,4},{7,5},{8,14},{9,15},{10,... | collective-permute-start | bytes 2359304 | tf_op jit(solution)/shard_map/ppermute | solution.py:347
  50.6 9.6 %collective-permute-start.18 = (bf16[48,2176]{1,0:T(8,128)(2,1)S(1)}, bf16[48,2176]{1,0:T(8,128)(2,1)S(1)}, u32[]{:S(2)}, u32[]{:S(2)}) collective-permute-start(bf16[48,2176]{1,0:T(8,128)(2,1)S(1)} %get-tuple-element.49), channel_id=1, source_target_pairs={{0,64},{8,72},{16,80},{24,88},{32,224},{40,232},{48,240},{56,248},... | collective-permute-start | bytes 626696 | tf_op jit(solution)/shard_map/ppermute | solution.py:422
  60.2 9.0 %collective-permute-start.19 = (bf16[48,2176]{1,0:T(8,128)(2,1)S(1)}, bf16[48,2176]{1,0:T(8,128)(2,1)S(1)}, u32[]{:S(2)}, u32[]{:S(2)}) collective-permute-start(bf16[48,2176]{1,0:T(8,128)(2,1)S(1)} %get-tuple-element.50), channel_id=1, source_target_pairs={{0,160},{8,168},{16,176},{24,184},{32,128},{40,136},{48,144},{56,1... | collective-permute-start | bytes 626696 | tf_op jit(solution)/shard_map/ppermute | solution.py:422
  69.2 25.1 %collective-permute-start.9 = (bf16[3072,128]{1,0:T(8,128)(2,1)S(1)}, bf16[3072,128]{1,0:T(8,128)(2,1)}, u32[]{:S(2)}, u32[]{:S(2)}) collective-permute-start(bf16[3072,128]{1,0:T(8,128)(2,1)S(1)} %copy-done.4), channel_id=1, source_target_pairs={{0,1},{1,0},{2,3},{3,2},{4,5},{5,4},{6,7},{7,6},{8,9},{9,8},{10,11... | collective-permute-start | bytes 2359304 | tf_op jit(solution)/shard_map/ppermute | solution.py:350
  74.6 20.1 %collective-permute-start.10 = (bf16[3072,128]{1,0:T(8,128)(2,1)}, bf16[3072,128]{1,0:T(8,128)(2,1)}, u32[]{:S(2)}, u32[]{:S(2)}) collective-permute-start(bf16[3072,128]{1,0:T(8,128)(2,1)} %get-tuple-element.45.refs_1_), channel_id=1, source_target_pairs={{0,1},{1,0},{2,3},{3,2},{4,5},{5,4},{6,7},{7,6},{8,9},{9,8},{10,11... | collective-permute-start | bytes 2359304 | tf_op jit(solution)/shard_map/ppermute | solution.py:350
  82.2 18.2 %collective-permute-start.7 = (bf16[3072,128]{1,0:T(8,128)(2,1)}, bf16[3072,128]{1,0:T(8,128)(2,1)}, u32[]{:S(2)}, u32[]{:S(2)}) collective-permute-start(bf16[3072,128]{1,0:T(8,128)(2,1)} %collective-permute-done.3.refs_2_), channel_id=1, source_target_pairs={{0,2},{1,3},{2,4},{3,5},{4,6},{5,7},{6,0},{7,1},{8,10},{9,11},{10,... | collective-permute-start | bytes 2359304 | tf_op jit(solution)/shard_map/ppermute | solution.py:347
  82.2 21.5 %collective-permute-start.8 = (bf16[3072,128]{1,0:T(8,128)(2,1)}, bf16[3072,128]{1,0:T(8,128)(2,1)}, u32[]{:S(2)}, u32[]{:S(2)}) collective-permute-start(bf16[3072,128]{1,0:T(8,128)(2,1)} %collective-permute-done.6.refs_5_), channel_id=1, source_target_pairs={{0,6},{1,7},{2,0},{3,1},{4,2},{5,3},{6,4},{7,5},{8,14},{9,15},{10,... | collective-permute-start | bytes 2359304 | tf_op jit(solution)/shard_map/ppermute | solution.py:347
  84.9 18.8 %collective-permute-start.11 = (bf16[3072,128]{1,0:T(8,128)(2,1)}, bf16[3072,128]{1,0:T(8,128)(2,1)}, u32[]{:S(2)}, u32[]{:S(2)}) collective-permute-start(bf16[3072,128]{1,0:T(8,128)(2,1)} %collective-permute-done.3.refs_2_), channel_id=1, source_target_pairs={{0,1},{1,0},{2,3},{3,2},{4,5},{5,4},{6,7},{7,6},{8,9},{9,8},{10,11... | collective-permute-start | bytes 2359304 | tf_op jit(solution)/shard_map/ppermute | solution.py:350
  89.4 29.1 %all-to-all-start.3 = ((bf16[8,24,2048]{2,1,0:T(8,128)(2,1)}), bf16[8,24,2048]{2,1,0:T(8,128)(2,1)S(1)}, u32[]{:S(2)}, u32[]{:S(2)}) async-start(bf16[8,24,2048]{2,1,0:T(8,128)(2,1)} %bitcast.13), calls=%async_computation.3 | async-start | bytes 1572864 | tf_op jit(solution)/shard_map/all_to_all | solution.py:427
  94.4 11.6 %collective-permute-start.14 = (bf16[3072,128]{1,0:T(8,128)(2,1)}, bf16[3072,128]{1,0:T(8,128)(2,1)S(1)}, u32[]{:S(2)}, u32[]{:S(2)}) collective-permute-start(bf16[3072,128]{1,0:T(8,128)(2,1)} %collective-permute-done.6.refs_5_), channel_id=1, source_target_pairs={{0,1},{1,0},{2,3},{3,2},{4,5},{5,4},{6,7},{7,6},{8,9},{9,8},{10,11... | collective-permute-start | bytes 2359304 | tf_op jit(solution)/shard_map/ppermute | solution.py:350
  94.7 9.6 %collective-permute-start.12 = (bf16[3072,128]{1,0:T(8,128)(2,1)}, bf16[3072,128]{1,0:T(8,128)(2,1)}, u32[]{:S(2)}, u32[]{:S(2)}) collective-permute-start(bf16[3072,128]{1,0:T(8,128)(2,1)} %collective-permute-done.4.refs_3_), channel_id=1, source_target_pairs={{0,1},{1,0},{2,3},{3,2},{4,5},{5,4},{6,7},{7,6},{8,9},{9,8},{10,11... | collective-permute-start | bytes 2359304 | tf_op jit(solution)/shard_map/ppermute | solution.py:350
  100.5 5.5 %collective-permute-start.13 = (bf16[3072,128]{1,0:T(8,128)(2,1)}, bf16[3072,128]{1,0:T(8,128)(2,1)}, u32[]{:S(2)}, u32[]{:S(2)}) collective-permute-start(bf16[3072,128]{1,0:T(8,128)(2,1)} %collective-permute-done.5.refs_4_), channel_id=1, source_target_pairs={{0,1},{1,0},{2,3},{3,2},{4,5},{5,4},{6,7},{7,6},{8,9},{9,8},{10,11... | collective-permute-start | bytes 2359304 | tf_op jit(solution)/shard_map/ppermute | solution.py:350
  103.7 3.4 %collective-permute-start.15 = (bf16[3072,128]{1,0:T(8,128)(2,1)}, bf16[3072,128]{1,0:T(8,128)(2,1)}, u32[]{:S(2)}, u32[]{:S(2)}) collective-permute-start(bf16[3072,128]{1,0:T(8,128)(2,1)} %collective-permute-done.7.refs_6_), channel_id=1, source_target_pairs={{0,1},{1,0},{2,3},{3,2},{4,5},{5,4},{6,7},{7,6},{8,9},{9,8},{10,11... | collective-permute-start | bytes 2359304 | tf_op jit(solution)/shard_map/ppermute | solution.py:350
  103.7 4.5 %collective-permute-start.16 = (bf16[3072,128]{1,0:T(8,128)(2,1)}, bf16[3072,128]{1,0:T(8,128)(2,1)}, u32[]{:S(2)}, u32[]{:S(2)}) collective-permute-start(bf16[3072,128]{1,0:T(8,128)(2,1)} %collective-permute-done.8.refs_7_), channel_id=1, source_target_pairs={{0,1},{1,0},{2,3},{3,2},{4,5},{5,4},{6,7},{7,6},{8,9},{9,8},{10,11... | collective-permute-start | bytes 2359304 | tf_op jit(solution)/shard_map/ppermute | solution.py:350
  106.0 2.2 %copy-start.5 = (bf16[3072,128]{1,0:T(8,128)(2,1)}, bf16[3072,128]{1,0:T(8,128)(2,1)S(1)}, u32[]{:S(2)}) copy-start(bf16[3072,128]{1,0:T(8,128)(2,1)S(1)} %collective-permute-done.14.refs_13_) | copy-start | bytes 2359300
  118.5 16.6 %all-to-all-start.2 = ((bf16[8,24,2048]{2,1,0:T(8,128)(2,1)}), bf16[8,24,2048]{2,1,0:T(8,128)(2,1)S(1)}, u32[]{:S(2)}, u32[]{:S(2)}) async-start(bf16[8,24,2048]{2,1,0:T(8,128)(2,1)} %bitcast.11), calls=%async_computation.2 | async-start | bytes 1572864 | tf_op jit(solution)/shard_map/all_to_all | solution.py:427
  133.5 46.4 %copy-start.6 = (f32[256]{0:T(256)S(1)}, f32[256]{0:T(256)}, u32[]{:S(2)}) copy-start(f32[256]{0:T(256)} %param.30) | copy-start | bytes 3076
  135.1 15.6 %all-to-all-start.4 = ((bf16[8,24,2048]{2,1,0:T(8,128)(2,1)}), bf16[8,24,2048]{2,1,0:T(8,128)(2,1)S(1)}, u32[]{:S(2)}, u32[]{:S(2)}) async-start(bf16[8,24,2048]{2,1,0:T(8,128)(2,1)} %bitcast.15), calls=%async_computation.4 | async-start | bytes 1572864 | tf_op jit(solution)/shard_map/all_to_all | solution.py:427
  139.5 17.0 %collective-permute-start.17 = (bf16[48,2048]{1,0:T(8,128)(2,1)S(1)}, bf16[48,2048]{1,0:T(8,128)(2,1)S(1)}, u32[]{:S(2)}, u32[]{:S(2)}) collective-permute-start(bf16[48,2048]{1,0:T(8,128)(2,1)S(1)} %get-tuple-element.48), channel_id=1, source_target_pairs={{0,224},{8,232},{16,240},{24,248},{32,64},{40,72},{48,80},{56,88},... | collective-permute-start | bytes 589832 | tf_op jit(solution)/shard_map/ppermute | solution.py:422
  151.1 8.0 %collective-permute-start.20 = (bf16[48,2048]{1,0:T(8,128)(2,1)S(1)}, bf16[48,2048]{1,0:T(8,128)(2,1)S(1)}, u32[]{:S(2)}, u32[]{:S(2)}) collective-permute-start(bf16[48,2048]{1,0:T(8,128)(2,1)S(1)} %get-tuple-element.53), channel_id=1, source_target_pairs={{0,192},{8,200},{16,208},{24,216},{32,96},{40,104},{48,112},{56,12... | collective-permute-start | bytes 589832 | tf_op jit(solution)/shard_map/ppermute | solution.py:422
  152.4 13.7 %collective-permute-start.21 = (bf16[48,2048]{1,0:T(8,128)(2,1)S(1)}, bf16[48,2048]{1,0:T(8,128)(2,1)S(1)}, u32[]{:S(2)}, u32[]{:S(2)}) collective-permute-start(bf16[48,2048]{1,0:T(8,128)(2,1)S(1)} %get-tuple-element.54), channel_id=1, source_target_pairs={{0,160},{8,168},{16,176},{24,184},{32,128},{40,136},{48,144},{56,1... | collective-permute-start | bytes 589832 | tf_op jit(solution)/shard_map/ppermute | solution.py:422
where the time goes:
time: 184 us; the launch traced here: 181 us
  starting transfers between devices  70.1 us (38%)
  waiting for transfers between devices  56.1 us (30%)
  Pallas kernels  37.3 us (20%)
  blocking collectives  13.3 us (7%)
  local copies, waits for them, and re-layouts  2.74 us (1%)
    pallas_call x9, Pallas kernels, kernel(): pl.pallas_call(body, out_shape=outs, in_specs=spaces, out_specs=[VMEM] *...  29.9 us
    ppermute x6, waiting for transfers between devices, along_z(): return lax.ppermute(array, 'sp', pairs)  25.6 us
    ppermute x6, starting transfers between devices, along_z(): return lax.ppermute(array, 'sp', pairs)  21.6 us
    all_to_all x4, starting transfers between devices, in_group(): lax.all_to_all(split, 'sp', 0, 0, axis_index_groups=groups, tiled=True)  17.2 us
    all_to_all x1, blocking collectives, layer(): last = lax.all_to_all(scaled, 'tp', 0, 0, tiled=True).reshape(ROWS, D // TP)  13.3 us
    ppermute x6, waiting for transfers between devices, along_y(): return lax.ppermute(array, 'tp', pairs)  13.1 us
    ppermute x8, starting transfers between devices, swapped(): return lax.ppermute(array, 'tp', [(n, n ^ 1) for n in range(TP)])  12.7 us
    all_to_all x4, waiting for transfers between devices, in_group(): lax.all_to_all(split, 'sp', 0, 0, axis_index_groups=groups, tiled=True)  11.3 us
  transfers between devices with their start and end apart: 27, of which 14 were waited for; matrix products, arithmetic and copies ran while one was open for 0% of the time, Pallas kernels for 15%

commit v1 on v0

--- a/solution.py
+++ b/solution.py
@@ -471,6 +471,10 @@
     back_one = shrink(made_one, tables_one)
     back = [*back_one, *back_two]
 
+    ret_near = along_z(back[1], -1, 1)
+    ret_other = along_z(back[2], -2, 2)
+    ret_far = along_z(back[3], -3, 3)
+
     (scaled,) = kernel(
         combine_kernel,
         16,
@@ -479,9 +483,9 @@
         normed,
         cols,
         back[0],
-        along_z(back[1], -1, 1),
-        along_z(back[2], -2, 2),
-        along_z(back[3], -3, 3),
+        ret_near,
+        ret_other,
+        ret_far,
     )
 
     last = lax.all_to_all(scaled, "tp", 0, 0, tiled=True).reshape(ROWS, D // TP)

time: 184 us -> 184 us (level)
  no operation moved by 1% of the time
where the time goes in v1:
time: 184 us; the launch traced here: 181 us
  starting transfers between devices  70.1 us (38%)
  waiting for transfers between devices  56.1 us (30%)
  Pallas kernels  37.3 us (20%)
  blocking collectives  13.3 us (7%)
  local copies, waits for them, and re-layouts  2.74 us (1%)
    pallas_call x9, Pallas kernels, kernel(): pl.pallas_call(body, out_shape=outs, in_specs=spaces, out_specs=[VMEM] *...  29.9 us
    ppermute x6, waiting for transfers between devices, along_z(): return lax.ppermute(array, 'sp', pairs)  25.6 us
    ppermute x6, starting transfers between devices, along_z(): return lax.ppermute(array, 'sp', pairs)  21.6 us
    all_to_all x4, starting transfers between devices, in_group(): lax.all_to_all(split, 'sp', 0, 0, axis_index_groups=groups, tiled=True)  17.2 us
    all_to_all x1, blocking collectives, layer(): last = lax.all_to_all(scaled, 'tp', 0, 0, tiled=True).reshape(ROWS, D // TP)  13.3 us
    ppermute x6, waiting for transfers between devices, along_y(): return lax.ppermute(array, 'tp', pairs)  13.1 us
    ppermute x8, starting transfers between devices, swapped(): return lax.ppermute(array, 'tp', [(n, n ^ 1) for n in range(TP)])  12.7 us
    all_to_all x4, waiting for transfers between devices, in_group(): lax.all_to_all(split, 'sp', 0, 0, axis_index_groups=groups, tiled=True)  11.3 us
  transfers between devices with their start and end apart: 27, of which 14 were waited for; matrix products, arithmetic and copies ran while one was open for 0% of the time, Pallas kernels for 15%

profile of v1, /device:TPU:1, one launch (start us, length us, event | category | flops | bytes accessed | tf_op | source)
XLA Modules:
  0.0 180.8 jit_solution(4707175581627271871)
XLA Ops:
  0.0 2.7 %pack.1 = (bf16[144,128]{1,0:T(8,128)(2,1)S(1)}, bf16[144,128]{1,0:T(8,128)(2,1)S(1)}, bf16[3072,128]{1,0:T(8,128)(2,1)}, bf16[3072,128]{1,0:T(8,128)(2,1)}, bf1...) custom-call(bf16[768,128]{1,0:T(8,128)(2,1)} %q.1, ...), custom_call_target="tpu_custom_call" | custom-call | tf_op jit(solution)/shard_map/pack/pallas_call | solution.py:331
  2.8 3.9 %collective-permute-start = (bf16[144,128]{1,0:T(8,128)(2,1)S(1)}, bf16[144,128]{1,0:T(8,128)(2,1)S(1)}, u32[]{:S(2)}, u32[]{:S(2)}) collective-permute-start(bf16[144,128]{1,0:T(8,128)(2,1)S(1)} %get-tuple-element.34), channel_id=1, source_target_pairs={{0,8},{8,16},{16,24},{24,32},{32,40},{40,48},{48,56},{56,64},{64,7... | collective-permute-start | bytes 110600 | tf_op jit(solution)/shard_map/ppermute | solution.py:342
  6.7 1.3 collective-permute-start.1
  8.0 0.0 copy-start.3
  8.0 0.6 copy-done.3
  8.7 2.4 %interior.1.part = bf16[768,128]{1,0:T(8,128)(2,1)S(1)} custom-call(f32[2]{0:T(128)S(1)} %copy-done.3, bf16[768,128]{1,0:T(8,128)(2,1)S(1)} %get-tuple-element.30.q, bf16[64,768]{1,0:T(8,128)(2,1)S(1)} %get-tuple-element.31.kt, bf16[64,768]{1,0:T(8,128)(2,1)S(1)} %get-tuple-element.32.vt, s32[6,128]{1,0:T(8,128)S(1)} %get-tuple-element.33.seg), custom_call_target="tpu_custom_call" | custom-call | tf_op jit(solution)/shard_map/interior/pallas_call | solution.py:365
  11.1 0.3 collective-permute-done.1.after
  11.4 2.3 %edges.1 = bf16[768,128]{1,0:T(8,128)(2,1)} custom-call(f32[2]{0:T(128)S(1)} %copy-done.3, bf16[768,128]{1,0:T(8,128)(2,1)S(1)} %get-tuple-element.30.q, bf16[64,768]{1,0:T(8,128)(2,1)S(1)} %get-tuple-element.31.kt, bf16[64,768]{1,0:T(8,128)(2,1)S(1)} %get-tuple-element.32.vt, s32[6,128]{1,0:T(8,128)S(1)} %get-tuple-element.33.seg, ...), custom_call_target="tpu_custom_call" | custom-call | tf_op jit(solution)/shard_map/edges/pallas_call | solution.py:394
  13.7 6.6 %all-to-all-start = ((bf16[8,96,128]{2,1,0:T(8,128)(2,1)}), bf16[8,96,128]{2,1,0:T(8,128)(2,1)S(1)}, u32[]{:S(2)}, u32[]{:S(2)}) async-start(bf16[8,96,128]{2,1,0:T(8,128)(2,1)} %bitcast.3), calls=%async_computation | async-start | bytes 393216 | tf_op jit(solution)/shard_map/all_to_all | solution.py:403
  20.3 0.7 reshape.42.group
  20.9 0.1 pad_add_fusion.where
  21.0 0.7 copy-done.1
  21.7 0.7 copy-done.2
  22.4 1.8 shard_map.154
  24.2 1.9 %all-to-all-done.att = bf16[8,96,128]{2,1,0:T(8,128)(2,1)S(1)} async-done(((bf16[8,96,128]{2,1,0:T(8,128)(2,1)}), bf16[8,96,128]{2,1,0:T(8,128)(2,1)S(1)}, u32[]{:S(2)}, u32[]{:S(2)}) %all-to-all-start) | async-done | bytes 196640 | tf_op jit(solution)/shard_map/all_to_all | solution.py:403
  26.1 3.1 %shard_map.155 = (bf16[96,2048]{1,0:T(8,128)(2,1)S(1)}, bf16[48,2176]{1,0:T(8,128)(2,1)S(1)}, bf16[48,2176]{1,0:T(8,128)(2,1)S(1)}, bf16[48,2176]{1,0:T(8,128)(2,1)S(1)}, bf16[48,2176]{1,0:T(8,128)(2,1)S(1)}) custom-call(bf16[8,96,128]{2,1,0:T(8,128)(2,1)S(1)} %all-to-all-done.att, bf16[1024,2048]{1,0:T(8,128)(2,1)} %weight.1, ...), custom_call_target="tpu_custom_call" | custom-call | tf_op jit(solution)/shard_map/pallas_call | solution.py:296
  29.3 7.5 %collective-permute-start.2 = (bf16[48,2176]{1,0:T(8,128)(2,1)S(1)}, bf16[48,2176]{1,0:T(8,128)(2,1)S(1)}, u32[]{:S(2)}, u32[]{:S(2)}) collective-permute-start(bf16[48,2176]{1,0:T(8,128)(2,1)S(1)} %get-tuple-element.42), channel_id=1, source_target_pairs={{0,224},{8,232},{16,240},{24,248},{32,64},{40,72},{48,80},{56,88},... | collective-permute-start | bytes 626696 | tf_op jit(solution)/shard_map/ppermute | solution.py:422
  36.7 4.6 %collective-permute-done.2.second = bf16[48,2176]{1,0:T(8,128)(2,1)S(1)} collective-permute-done((bf16[48,2176]{1,0:T(8,128)(2,1)S(1)}, bf16[48,2176]{1,0:T(8,128)(2,1)S(1)}, u32[]{:S(2)}, u32[]{:S(2)}) %collective-permute-start.2) | collective-permute-done | bytes 208928 | tf_op jit(solution)/shard_map/ppermute | solution.py:422
  41.3 1.5 shard_map.156
  42.9 3.5 %all-to-all-start.1 = ((bf16[8,24,2048]{2,1,0:T(8,128)(2,1)}), bf16[8,24,2048]{2,1,0:T(8,128)(2,1)S(1)}, u32[]{:S(2)}, u32[]{:S(2)}) async-start(bf16[8,24,2048]{2,1,0:T(8,128)(2,1)} %bitcast.9), calls=%async_computation.1 | async-start | bytes 1572864 | tf_op jit(solution)/shard_map/all_to_all | solution.py:427
  46.4 0.3 collective-permute-start.3
  46.8 1.0 collective-permute-start.4
  47.8 1.6 collective-permute-start.6
  49.4 1.2 collective-permute-start.5
  50.6 4.4 %collective-permute-start.18 = (bf16[48,2176]{1,0:T(8,128)(2,1)S(1)}, bf16[48,2176]{1,0:T(8,128)(2,1)S(1)}, u32[]{:S(2)}, u32[]{:S(2)}) collective-permute-start(bf16[48,2176]{1,0:T(8,128)(2,1)S(1)} %get-tuple-element.49), channel_id=1, source_target_pairs={{0,64},{8,72},{16,80},{24,88},{32,224},{40,232},{48,240},{56,248},... | collective-permute-start | bytes 626696 | tf_op jit(solution)/shard_map/ppermute | solution.py:422
  55.0 5.2 %collective-permute-done.18.first = bf16[48,2176]{1,0:T(8,128)(2,1)S(1)} collective-permute-done((bf16[48,2176]{1,0:T(8,128)(2,1)S(1)}, bf16[48,2176]{1,0:T(8,128)(2,1)S(1)}, u32[]{:S(2)}, u32[]{:S(2)}) %collective-permute-start.18) | collective-permute-done | bytes 208928 | tf_op jit(solution)/shard_map/ppermute | solution.py:422
  60.2 2.8 %collective-permute-start.19 = (bf16[48,2176]{1,0:T(8,128)(2,1)S(1)}, bf16[48,2176]{1,0:T(8,128)(2,1)S(1)}, u32[]{:S(2)}, u32[]{:S(2)}) collective-permute-start(bf16[48,2176]{1,0:T(8,128)(2,1)S(1)} %get-tuple-element.50), channel_id=1, source_target_pairs={{0,160},{8,168},{16,176},{24,184},{32,128},{40,136},{48,144},{56,1... | collective-permute-start | bytes 626696 | tf_op jit(solution)/shard_map/ppermute | solution.py:422
  63.0 6.2 %collective-permute-done.19.second = bf16[48,2176]{1,0:T(8,128)(2,1)S(1)} collective-permute-done((bf16[48,2176]{1,0:T(8,128)(2,1)S(1)}, bf16[48,2176]{1,0:T(8,128)(2,1)S(1)}, u32[]{:S(2)}, u32[]{:S(2)}) %collective-permute-start.19) | collective-permute-done | bytes 208928 | tf_op jit(solution)/shard_map/ppermute | solution.py:422
  69.2 5.4 %collective-permute-start.9 = (bf16[3072,128]{1,0:T(8,128)(2,1)S(1)}, bf16[3072,128]{1,0:T(8,128)(2,1)}, u32[]{:S(2)}, u32[]{:S(2)}) collective-permute-start(bf16[3072,128]{1,0:T(8,128)(2,1)S(1)} %copy-done.4), channel_id=1, source_target_pairs={{0,1},{1,0},{2,3},{3,2},{4,5},{5,4},{6,7},{7,6},{8,9},{9,8},{10,11... | collective-permute-start | bytes 2359304 | tf_op jit(solution)/shard_map/ppermute | solution.py:350
  74.6 0.0 collective-permute-done.3.refs_2_
  74.6 0.0 collective-permute-start.10
  74.6 7.6 %collective-permute-done.4.refs_3_ = bf16[3072,128]{1,0:T(8,128)(2,1)} collective-permute-done((bf16[3072,128]{1,0:T(8,128)(2,1)}, bf16[3072,128]{1,0:T(8,128)(2,1)}, u32[]{:S(2)}, u32[]{:S(2)}) %collective-permute-start.4) | collective-permute-done | bytes 786464 | tf_op jit(solution)/shard_map/ppermute | solution.py:347
  82.2 0.0 collective-permute-start.7
  82.2 2.7 %collective-permute-start.8 = (bf16[3072,128]{1,0:T(8,128)(2,1)}, bf16[3072,128]{1,0:T(8,128)(2,1)}, u32[]{:S(2)}, u32[]{:S(2)}) collective-permute-start(bf16[3072,128]{1,0:T(8,128)(2,1)} %collective-permute-done.6.refs_5_), channel_id=1, source_target_pairs={{0,6},{1,7},{2,0},{3,1},{4,2},{5,3},{6,4},{7,5},{8,14},{9,15},{10,... | collective-permute-start | bytes 2359304 | tf_op jit(solution)/shard_map/ppermute | solution.py:347
  84.9 2.9 %collective-permute-start.11 = (bf16[3072,128]{1,0:T(8,128)(2,1)}, bf16[3072,128]{1,0:T(8,128)(2,1)}, u32[]{:S(2)}, u32[]{:S(2)}) collective-permute-start(bf16[3072,128]{1,0:T(8,128)(2,1)} %collective-permute-done.3.refs_2_), channel_id=1, source_target_pairs={{0,1},{1,0},{2,3},{3,2},{4,5},{5,4},{6,7},{7,6},{8,9},{9,8},{10,11... | collective-permute-start | bytes 2359304 | tf_op jit(solution)/shard_map/ppermute | solution.py:350
  87.9 1.5 shard_map.159
  89.4 5.0 %all-to-all-start.3 = ((bf16[8,24,2048]{2,1,0:T(8,128)(2,1)}), bf16[8,24,2048]{2,1,0:T(8,128)(2,1)S(1)}, u32[]{:S(2)}, u32[]{:S(2)}) async-start(bf16[8,24,2048]{2,1,0:T(8,128)(2,1)} %bitcast.13), calls=%async_computation.3 | async-start | bytes 1572864 | tf_op jit(solution)/shard_map/all_to_all | solution.py:427
  94.4 0.4 collective-permute-start.14
  94.7 0.2 collective-permute-start.12
  95.0 5.5 %collective-permute-done.7.refs_6_ = bf16[3072,128]{1,0:T(8,128)(2,1)} collective-permute-done((bf16[3072,128]{1,0:T(8,128)(2,1)}, bf16[3072,128]{1,0:T(8,128)(2,1)}, u32[]{:S(2)}, u32[]{:S(2)}) %collective-permute-start.7) | collective-permute-done | bytes 786464 | tf_op jit(solution)/shard_map/ppermute | solution.py:347
  100.5 3.2 %collective-permute-start.13 = (bf16[3072,128]{1,0:T(8,128)(2,1)}, bf16[3072,128]{1,0:T(8,128)(2,1)}, u32[]{:S(2)}, u32[]{:S(2)}) collective-permute-start(bf16[3072,128]{1,0:T(8,128)(2,1)} %collective-permute-done.5.refs_4_), channel_id=1, source_target_pairs={{0,1},{1,0},{2,3},{3,2},{4,5},{5,4},{6,7},{7,6},{8,9},{9,8},{10,11... | collective-permute-start | bytes 2359304 | tf_op jit(solution)/shard_map/ppermute | solution.py:350
  103.7 0.0 collective-permute-start.15
  103.7 0.5 collective-permute-start.16
  104.2 0.1 add_and_fusion.order
  104.3 1.6 collective-permute-done.13.refs_12_
  106.0 1.1 collective-permute-done.15.refs_14_
  107.1 1.1 collective-permute-done.16.refs_15_
  108.2 10.3 %shard_map.157 = bf16[192,2048]{1,0:T(8,128)(2,1)} custom-call(s32[8]{0:T(128)S(1)} %add_and_fusion.order, bf16[192,2048]{1,0:T(8,128)(2,1)S(1)} %bitcast.20, bf16[3072,128]{1,0:T(8,128)(2,1)} %get-tuple-element.44.refs_0_, bf16[3072,128]{1,0:T(8,128)(2,1)} %get-tuple-element.45.refs_1_, bf16[3072,128]{1,0:T(8,128)(2,1)} %collective-permute-done.3.refs_2_, ...), custom_call_target="tpu_custom_call" | custom-call | tf_op jit(solution)/shard_map/pallas_call | solution.py:296
  118.5 4.7 %all-to-all-start.2 = ((bf16[8,24,2048]{2,1,0:T(8,128)(2,1)}), bf16[8,24,2048]{2,1,0:T(8,128)(2,1)S(1)}, u32[]{:S(2)}, u32[]{:S(2)}) async-start(bf16[8,24,2048]{2,1,0:T(8,128)(2,1)} %bitcast.11), calls=%async_computation.2 | async-start | bytes 1572864 | tf_op jit(solution)/shard_map/all_to_all | solution.py:427
  123.2 10.3 %shard_map.160 = bf16[192,2048]{1,0:T(8,128)(2,1)} custom-call(s32[8]{0:T(128)S(1)} %add_and_fusion.order, bf16[192,2048]{1,0:T(8,128)(2,1)S(1)} %bitcast.21, bf16[3072,128]{1,0:T(8,128)(2,1)} %get-tuple-element.44.refs_0_, bf16[3072,128]{1,0:T(8,128)(2,1)} %get-tuple-element.45.refs_1_, bf16[3072,128]{1,0:T(8,128)(2,1)} %collective-permute-done.3.refs_2_, ...), custom_call_target="tpu_custom_call" | custom-call | tf_op jit(solution)/shard_map/pallas_call | solution.py:296
  133.5 0.0 copy-start.6
  133.5 1.6 all-to-all-done.2
  135.1 4.0 %all-to-all-start.4 = ((bf16[8,24,2048]{2,1,0:T(8,128)(2,1)}), bf16[8,24,2048]{2,1,0:T(8,128)(2,1)S(1)}, u32[]{:S(2)}, u32[]{:S(2)}) async-start(bf16[8,24,2048]{2,1,0:T(8,128)(2,1)} %bitcast.15), calls=%async_computation.4 | async-start | bytes 1572864 | tf_op jit(solution)/shard_map/all_to_all | solution.py:427
  139.0 0.4 shard_map.158
  139.5 1.5 collective-permute-start.17
  141.0 9.7 %all-to-all-done.4 = bf16[8,24,2048]{2,1,0:T(8,128)(2,1)S(1)} async-done(((bf16[8,24,2048]{2,1,0:T(8,128)(2,1)}), bf16[8,24,2048]{2,1,0:T(8,128)(2,1)S(1)}, u32[]{:S(2)}, u32[]{:S(2)}) %all-to-all-start.4) | async-done | bytes 786464 | tf_op jit(solution)/shard_map/all_to_all | solution.py:427
  150.7 0.4 shard_map.161
  151.1 1.2 collective-permute-start.20
  152.4 4.1 %collective-permute-start.21 = (bf16[48,2048]{1,0:T(8,128)(2,1)S(1)}, bf16[48,2048]{1,0:T(8,128)(2,1)S(1)}, u32[]{:S(2)}, u32[]{:S(2)}) collective-permute-start(bf16[48,2048]{1,0:T(8,128)(2,1)S(1)} %get-tuple-element.54), channel_id=1, source_target_pairs={{0,160},{8,168},{16,176},{24,184},{32,128},{40,136},{48,144},{56,1... | collective-permute-start | bytes 589832 | tf_op jit(solution)/shard_map/ppermute | solution.py:422
  156.5 2.6 %collective-permute-done.20.b = bf16[48,2048]{1,0:T(8,128)(2,1)S(1)} collective-permute-done((bf16[48,2048]{1,0:T(8,128)(2,1)S(1)}, bf16[48,2048]{1,0:T(8,128)(2,1)S(1)}, u32[]{:S(2)}, u32[]{:S(2)}) %collective-permute-start.20) | collective-permute-done | bytes 196640 | tf_op jit(solution)/shard_map/ppermute | solution.py:422
  159.1 7.0 %collective-permute-done.21.c = bf16[48,2048]{1,0:T(8,128)(2,1)S(1)} collective-permute-done((bf16[48,2048]{1,0:T(8,128)(2,1)S(1)}, bf16[48,2048]{1,0:T(8,128)(2,1)S(1)}, u32[]{:S(2)}, u32[]{:S(2)}) %collective-permute-start.21) | collective-permute-done | bytes 196640 | tf_op jit(solution)/shard_map/ppermute | solution.py:422
  166.1 0.6 shard_map.162
  166.7 13.3 %all_to_all.30 = bf16[8,96,256]{2,1,0:T(8,128)(2,1)S(1)} all-to-all(bf16[8,96,256]{2,1,0:T(8,128)(2,1)S(1)} %shard_map.162), channel_id=1, replica_groups=mesh['sp'=32,'tp'=8] {'tp'}, dimensions={0} | all-to-all | bytes 786432 | tf_op jit(solution)/shard_map/all_to_all | solution.py:491
  179.9 0.8 fusion
  (24 shorter events, 0.1 us)
Async XLA Ops:
  0.0 26.1 %copy-start = (f32[2048]{0:T(1024)S(1)}, f32[2048]{0:T(1024)}, u32[]{:S(2)}) copy-start(f32[2048]{0:T(1024)} %param.23) | copy-start | bytes 24580
  2.8 8.3 %collective-permute-start = (bf16[144,128]{1,0:T(8,128)(2,1)S(1)}, bf16[144,128]{1,0:T(8,128)(2,1)S(1)}, u32[]{:S(2)}, u32[]{:S(2)}) collective-permute-start(bf16[144,128]{1,0:T(8,128)(2,1)S(1)} %get-tuple-element.34), channel_id=1, source_target_pairs={{0,8},{8,16},{16,24},{24,32},{32,40},{40,48},{48,56},{56,64},{64,7... | collective-permute-start | bytes 110600 | tf_op jit(solution)/shard_map/ppermute | solution.py:342
  6.7 4.7 %collective-permute-start.1 = (bf16[144,128]{1,0:T(8,128)(2,1)S(1)}, bf16[144,128]{1,0:T(8,128)(2,1)S(1)}, u32[]{:S(2)}, u32[]{:S(2)}) collective-permute-start(bf16[144,128]{1,0:T(8,128)(2,1)S(1)} %get-tuple-element.35), channel_id=1, source_target_pairs={{8,0},{16,8},{24,16},{32,24},{40,32},{48,40},{56,48},{64,56},{72,6... | collective-permute-start | bytes 110600 | tf_op jit(solution)/shard_map/ppermute | solution.py:343
  8.0 0.7 copy-start.3
  13.7 12.4 %all-to-all-start = ((bf16[8,96,128]{2,1,0:T(8,128)(2,1)}), bf16[8,96,128]{2,1,0:T(8,128)(2,1)S(1)}, u32[]{:S(2)}, u32[]{:S(2)}) async-start(bf16[8,96,128]{2,1,0:T(8,128)(2,1)} %bitcast.3), calls=%async_computation | async-start | bytes 393216 | tf_op jit(solution)/shard_map/all_to_all | solution.py:403
  21.0 0.7 copy-start.1
  21.7 0.7 copy-start.2
  24.2 22.2 %copy-start.4 = (bf16[3072,128]{1,0:T(8,128)(2,1)S(1)}, bf16[3072,128]{1,0:T(8,128)(2,1)}, u32[]{:S(2)}) copy-start(bf16[3072,128]{1,0:T(8,128)(2,1)} %get-tuple-element.44.refs_0_) | copy-start | bytes 2359300
  26.1 78.1 %copy-start.7 = (s32[4]{0:T(128)S(1)}, s32[4]{0:T(128)}, u32[]{:S(2)}) copy-start(s32[4]{0:T(128)} %constant.17.clone) | copy-start | bytes 52
  29.3 12.1 %collective-permute-start.2 = (bf16[48,2176]{1,0:T(8,128)(2,1)S(1)}, bf16[48,2176]{1,0:T(8,128)(2,1)S(1)}, u32[]{:S(2)}, u32[]{:S(2)}) collective-permute-start(bf16[48,2176]{1,0:T(8,128)(2,1)S(1)} %get-tuple-element.42), channel_id=1, source_target_pairs={{0,224},{8,232},{16,240},{24,248},{32,64},{40,72},{48,80},{56,88},... | collective-permute-start | bytes 626696 | tf_op jit(solution)/shard_map/ppermute | solution.py:422
  42.9 46.5 %all-to-all-start.1 = ((bf16[8,24,2048]{2,1,0:T(8,128)(2,1)}), bf16[8,24,2048]{2,1,0:T(8,128)(2,1)S(1)}, u32[]{:S(2)}, u32[]{:S(2)}) async-start(bf16[8,24,2048]{2,1,0:T(8,128)(2,1)} %bitcast.9), calls=%async_computation.1 | async-start | bytes 1572864 | tf_op jit(solution)/shard_map/all_to_all | solution.py:427
  46.4 28.2 %collective-permute-start.3 = (bf16[3072,128]{1,0:T(8,128)(2,1)S(1)}, bf16[3072,128]{1,0:T(8,128)(2,1)}, u32[]{:S(2)}, u32[]{:S(2)}) collective-permute-start(bf16[3072,128]{1,0:T(8,128)(2,1)S(1)} %copy-done.4), channel_id=1, source_target_pairs={{0,2},{1,3},{2,4},{3,5},{4,6},{5,7},{6,0},{7,1},{8,10},{9,11},{10,... | collective-permute-start | bytes 2359304 | tf_op jit(solution)/shard_map/ppermute | solution.py:347
  46.8 35.5 %collective-permute-start.4 = (bf16[3072,128]{1,0:T(8,128)(2,1)}, bf16[3072,128]{1,0:T(8,128)(2,1)}, u32[]{:S(2)}, u32[]{:S(2)}) collective-permute-start(bf16[3072,128]{1,0:T(8,128)(2,1)} %get-tuple-element.45.refs_1_), channel_id=1, source_target_pairs={{0,2},{1,3},{2,4},{3,5},{4,6},{5,7},{6,0},{7,1},{8,10},{9,11},{10,... | collective-permute-start | bytes 2359304 | tf_op jit(solution)/shard_map/ppermute | solution.py:347
  47.8 34.5 %collective-permute-start.6 = (bf16[3072,128]{1,0:T(8,128)(2,1)}, bf16[3072,128]{1,0:T(8,128)(2,1)}, u32[]{:S(2)}, u32[]{:S(2)}) collective-permute-start(bf16[3072,128]{1,0:T(8,128)(2,1)} %get-tuple-element.45.refs_1_), channel_id=1, source_target_pairs={{0,6},{1,7},{2,0},{3,1},{4,2},{5,3},{6,4},{7,5},{8,14},{9,15},{10,... | collective-permute-start | bytes 2359304 | tf_op jit(solution)/shard_map/ppermute | solution.py:347
  49.4 35.5 %collective-permute-start.5 = (bf16[3072,128]{1,0:T(8,128)(2,1)S(1)}, bf16[3072,128]{1,0:T(8,128)(2,1)}, u32[]{:S(2)}, u32[]{:S(2)}) collective-permute-start(bf16[3072,128]{1,0:T(8,128)(2,1)S(1)} %copy-done.4), channel_id=1, source_target_pairs={{0,6},{1,7},{2,0},{3,1},{4,2},{5,3},{6,4},{7,5},{8,14},{9,15},{10,... | collective-permute-start | bytes 2359304 | tf_op jit(solution)/shard_map/ppermute | solution.py:347
  50.6 9.6 %collective-permute-start.18 = (bf16[48,2176]{1,0:T(8,128)(2,1)S(1)}, bf16[48,2176]{1,0:T(8,128)(2,1)S(1)}, u32[]{:S(2)}, u32[]{:S(2)}) collective-permute-start(bf16[48,2176]{1,0:T(8,128)(2,1)S(1)} %get-tuple-element.49), channel_id=1, source_target_pairs={{0,64},{8,72},{16,80},{24,88},{32,224},{40,232},{48,240},{56,248},... | collective-permute-start | bytes 626696 | tf_op jit(solution)/shard_map/ppermute | solution.py:422
  60.2 9.0 %collective-permute-start.19 = (bf16[48,2176]{1,0:T(8,128)(2,1)S(1)}, bf16[48,2176]{1,0:T(8,128)(2,1)S(1)}, u32[]{:S(2)}, u32[]{:S(2)}) collective-permute-start(bf16[48,2176]{1,0:T(8,128)(2,1)S(1)} %get-tuple-element.50), channel_id=1, source_target_pairs={{0,160},{8,168},{16,176},{24,184},{32,128},{40,136},{48,144},{56,1... | collective-permute-start | bytes 626696 | tf_op jit(solution)/shard_map/ppermute | solution.py:422
  69.2 25.1 %collective-permute-start.9 = (bf16[3072,128]{1,0:T(8,128)(2,1)S(1)}, bf16[3072,128]{1,0:T(8,128)(2,1)}, u32[]{:S(2)}, u32[]{:S(2)}) collective-permute-start(bf16[3072,128]{1,0:T(8,128)(2,1)S(1)} %copy-done.4), channel_id=1, source_target_pairs={{0,1},{1,0},{2,3},{3,2},{4,5},{5,4},{6,7},{7,6},{8,9},{9,8},{10,11... | collective-permute-start | bytes 2359304 | tf_op jit(solution)/shard_map/ppermute | solution.py:350
  74.6 20.1 %collective-permute-start.10 = (bf16[3072,128]{1,0:T(8,128)(2,1)}, bf16[3072,128]{1,0:T(8,128)(2,1)}, u32[]{:S(2)}, u32[]{:S(2)}) collective-permute-start(bf16[3072,128]{1,0:T(8,128)(2,1)} %get-tuple-element.45.refs_1_), channel_id=1, source_target_pairs={{0,1},{1,0},{2,3},{3,2},{4,5},{5,4},{6,7},{7,6},{8,9},{9,8},{10,11... | collective-permute-start | bytes 2359304 | tf_op jit(solution)/shard_map/ppermute | solution.py:350
  82.2 18.2 %collective-permute-start.7 = (bf16[3072,128]{1,0:T(8,128)(2,1)}, bf16[3072,128]{1,0:T(8,128)(2,1)}, u32[]{:S(2)}, u32[]{:S(2)}) collective-permute-start(bf16[3072,128]{1,0:T(8,128)(2,1)} %collective-permute-done.3.refs_2_), channel_id=1, source_target_pairs={{0,2},{1,3},{2,4},{3,5},{4,6},{5,7},{6,0},{7,1},{8,10},{9,11},{10,... | collective-permute-start | bytes 2359304 | tf_op jit(solution)/shard_map/ppermute | solution.py:347
  82.2 21.5 %collective-permute-start.8 = (bf16[3072,128]{1,0:T(8,128)(2,1)}, bf16[3072,128]{1,0:T(8,128)(2,1)}, u32[]{:S(2)}, u32[]{:S(2)}) collective-permute-start(bf16[3072,128]{1,0:T(8,128)(2,1)} %collective-permute-done.6.refs_5_), channel_id=1, source_target_pairs={{0,6},{1,7},{2,0},{3,1},{4,2},{5,3},{6,4},{7,5},{8,14},{9,15},{10,... | collective-permute-start | bytes 2359304 | tf_op jit(solution)/shard_map/ppermute | solution.py:347
  84.9 18.8 %collective-permute-start.11 = (bf16[3072,128]{1,0:T(8,128)(2,1)}, bf16[3072,128]{1,0:T(8,128)(2,1)}, u32[]{:S(2)}, u32[]{:S(2)}) collective-permute-start(bf16[3072,128]{1,0:T(8,128)(2,1)} %collective-permute-done.3.refs_2_), channel_id=1, source_target_pairs={{0,1},{1,0},{2,3},{3,2},{4,5},{5,4},{6,7},{7,6},{8,9},{9,8},{10,11... | collective-permute-start | bytes 2359304 | tf_op jit(solution)/shard_map/ppermute | solution.py:350
  89.4 29.1 %all-to-all-start.3 = ((bf16[8,24,2048]{2,1,0:T(8,128)(2,1)}), bf16[8,24,2048]{2,1,0:T(8,128)(2,1)S(1)}, u32[]{:S(2)}, u32[]{:S(2)}) async-start(bf16[8,24,2048]{2,1,0:T(8,128)(2,1)} %bitcast.13), calls=%async_computation.3 | async-start | bytes 1572864 | tf_op jit(solution)/shard_map/all_to_all | solution.py:427
  94.4 11.6 %collective-permute-start.14 = (bf16[3072,128]{1,0:T(8,128)(2,1)}, bf16[3072,128]{1,0:T(8,128)(2,1)S(1)}, u32[]{:S(2)}, u32[]{:S(2)}) collective-permute-start(bf16[3072,128]{1,0:T(8,128)(2,1)} %collective-permute-done.6.refs_5_), channel_id=1, source_target_pairs={{0,1},{1,0},{2,3},{3,2},{4,5},{5,4},{6,7},{7,6},{8,9},{9,8},{10,11... | collective-permute-start | bytes 2359304 | tf_op jit(solution)/shard_map/ppermute | solution.py:350
  94.7 9.6 %collective-permute-start.12 = (bf16[3072,128]{1,0:T(8,128)(2,1)}, bf16[3072,128]{1,0:T(8,128)(2,1)}, u32[]{:S(2)}, u32[]{:S(2)}) collective-permute-start(bf16[3072,128]{1,0:T(8,128)(2,1)} %collective-permute-done.4.refs_3_), channel_id=1, source_target_pairs={{0,1},{1,0},{2,3},{3,2},{4,5},{5,4},{6,7},{7,6},{8,9},{9,8},{10,11... | collective-permute-start | bytes 2359304 | tf_op jit(solution)/shard_map/ppermute | solution.py:350
  100.5 5.5 %collective-permute-start.13 = (bf16[3072,128]{1,0:T(8,128)(2,1)}, bf16[3072,128]{1,0:T(8,128)(2,1)}, u32[]{:S(2)}, u32[]{:S(2)}) collective-permute-start(bf16[3072,128]{1,0:T(8,128)(2,1)} %collective-permute-done.5.refs_4_), channel_id=1, source_target_pairs={{0,1},{1,0},{2,3},{3,2},{4,5},{5,4},{6,7},{7,6},{8,9},{9,8},{10,11... | collective-permute-start | bytes 2359304 | tf_op jit(solution)/shard_map/ppermute | solution.py:350
  103.7 3.4 %collective-permute-start.15 = (bf16[3072,128]{1,0:T(8,128)(2,1)}, bf16[3072,128]{1,0:T(8,128)(2,1)}, u32[]{:S(2)}, u32[]{:S(2)}) collective-permute-start(bf16[3072,128]{1,0:T(8,128)(2,1)} %collective-permute-done.7.refs_6_), channel_id=1, source_target_pairs={{0,1},{1,0},{2,3},{3,2},{4,5},{5,4},{6,7},{7,6},{8,9},{9,8},{10,11... | collective-permute-start | bytes 2359304 | tf_op jit(solution)/shard_map/ppermute | solution.py:350
  103.7 4.5 %collective-permute-start.16 = (bf16[3072,128]{1,0:T(8,128)(2,1)}, bf16[3072,128]{1,0:T(8,128)(2,1)}, u32[]{:S(2)}, u32[]{:S(2)}) collective-permute-start(bf16[3072,128]{1,0:T(8,128)(2,1)} %collective-permute-done.8.refs_7_), channel_id=1, source_target_pairs={{0,1},{1,0},{2,3},{3,2},{4,5},{5,4},{6,7},{7,6},{8,9},{9,8},{10,11... | collective-permute-start | bytes 2359304 | tf_op jit(solution)/shard_map/ppermute | solution.py:350
  106.0 2.2 %copy-start.5 = (bf16[3072,128]{1,0:T(8,128)(2,1)}, bf16[3072,128]{1,0:T(8,128)(2,1)S(1)}, u32[]{:S(2)}) copy-start(bf16[3072,128]{1,0:T(8,128)(2,1)S(1)} %collective-permute-done.14.refs_13_) | copy-start | bytes 2359300
  118.5 16.6 %all-to-all-start.2 = ((bf16[8,24,2048]{2,1,0:T(8,128)(2,1)}), bf16[8,24,2048]{2,1,0:T(8,128)(2,1)S(1)}, u32[]{:S(2)}, u32[]{:S(2)}) async-start(bf16[8,24,2048]{2,1,0:T(8,128)(2,1)} %bitcast.11), calls=%async_computation.2 | async-start | bytes 1572864 | tf_op jit(solution)/shard_map/all_to_all | solution.py:427
  133.5 46.4 %copy-start.6 = (f32[256]{0:T(256)S(1)}, f32[256]{0:T(256)}, u32[]{:S(2)}) copy-start(f32[256]{0:T(256)} %param.30) | copy-start | bytes 3076
  135.1 15.6 %all-to-all-start.4 = ((bf16[8,24,2048]{2,1,0:T(8,128)(2,1)}), bf16[8,24,2048]{2,1,0:T(8,128)(2,1)S(1)}, u32[]{:S(2)}, u32[]{:S(2)}) async-start(bf16[8,24,2048]{2,1,0:T(8,128)(2,1)} %bitcast.15), calls=%async_computation.4 | async-start | bytes 1572864 | tf_op jit(solution)/shard_map/all_to_all | solution.py:427
  139.5 17.0 %collective-permute-start.17 = (bf16[48,2048]{1,0:T(8,128)(2,1)S(1)}, bf16[48,2048]{1,0:T(8,128)(2,1)S(1)}, u32[]{:S(2)}, u32[]{:S(2)}) collective-permute-start(bf16[48,2048]{1,0:T(8,128)(2,1)S(1)} %get-tuple-element.48), channel_id=1, source_target_pairs={{0,224},{8,232},{16,240},{24,248},{32,64},{40,72},{48,80},{56,88},... | collective-permute-start | bytes 589832 | tf_op jit(solution)/shard_map/ppermute | solution.py:422
  151.1 8.0 %collective-permute-start.20 = (bf16[48,2048]{1,0:T(8,128)(2,1)S(1)}, bf16[48,2048]{1,0:T(8,128)(2,1)S(1)}, u32[]{:S(2)}, u32[]{:S(2)}) collective-permute-start(bf16[48,2048]{1,0:T(8,128)(2,1)S(1)} %get-tuple-element.53), channel_id=1, source_target_pairs={{0,192},{8,200},{16,208},{24,216},{32,96},{40,104},{48,112},{56,12... | collective-permute-start | bytes 589832 | tf_op jit(solution)/shard_map/ppermute | solution.py:422
  152.4 13.7 %collective-permute-start.21 = (bf16[48,2048]{1,0:T(8,128)(2,1)S(1)}, bf16[48,2048]{1,0:T(8,128)(2,1)S(1)}, u32[]{:S(2)}, u32[]{:S(2)}) collective-permute-start(bf16[48,2048]{1,0:T(8,128)(2,1)S(1)} %get-tuple-element.54), channel_id=1, source_target_pairs={{0,160},{8,168},{16,176},{24,184},{32,128},{40,136},{48,144},{56,1... | collective-permute-start | bytes 589832 | tf_op jit(solution)/shard_map/ppermute | solution.py:422
